TPU v7x, 32 devices: a whole 2x2x4 slice. The times are simulated.
32 devices in a mesh: sp: 8 (over z, y), tp: 4 (over x, core).
Axes of the slice: x: 2, y: 2, z: 4, core: 2. Of those that a mesh axis runs over, the one named last changes fastest.
Arguments:
- hidden_state: bfloat16 [1024, 2048], P('sp'), may hold values from -125 to 125
- norm_gain: float32 [2048], replicated, may hold values from 0.1 to 1.9
- route_ids: int32 [1024, 2], P('sp'), may hold values from 0 to 7, all different within a row; in each aligned block of 128 rows (0 to 127, 128 to 255, ...) at most 64 rows name the same one
- route_logits: float32 [1024, 2], P('sp'), may hold values from -6 to 6
- cotangent: bfloat16 [1024, 2048], P('sp'), may hold values from -6 to 6
- w_gate: bfloat16 [8, 2048, 1536], P('sp', None, 'tp'), may hold values from -0.125 to 0.125
- w_up: bfloat16 [8, 2048, 1536], P('sp', None, 'tp'), may hold values from -0.125 to 0.125
- w_down: bfloat16 [8, 1536, 2048], P('sp', 'tp'), may hold values from -0.15625 to 0.15625
- w_out: bfloat16 [2048, 1024], P(None, 'tp'), may hold values from -0.1875 to 0.1875
- query_rows: bfloat16 [1024, 512], P('sp', 'tp'), may hold values from -6 to 6
- key_rows: bfloat16 [1024, 512], P('sp', 'tp'), may hold values from -6 to 6
- value_rows: bfloat16 [1024, 1024], P('sp', 'tp'), may hold values from -6 to 6
- log_decay: float32 [1024, 512], P('sp', 'tp'), may hold values from -1.6 to 0
- head_gain: float32 [1024], P('tp'), may hold values from 0.1 to 1.9
Outputs:
- d_w_gate: bfloat16 [8, 2048, 1536], P('sp', None, 'tp')
- d_w_up: bfloat16 [8, 2048, 1536], P('sp', None, 'tp')
- d_w_down: bfloat16 [8, 1536, 2048], P('sp', 'tp')
- d_w_out: float32 [2048, 1024], P('sp', 'tp')
- d_queries: bfloat16 [1024, 512], P('sp', 'tp')
- d_keys: bfloat16 [1024, 512], P('sp', 'tp')
- d_values: bfloat16 [1024, 1024], P('sp', 'tp')
- d_log_decay: float32 [1024, 512], P('sp', 'tp')
Inputs may be any that keep to these rules, and one draw needn't show every extreme that they name: `route_ids`: in the rows of one device each expert is named at most 64 times, a bound that some block reaches; the two experts of a position differ.
All inputs are finite; a program needn't handle non-finite values.
Results may differ from a plain program's by a relative error of at most 0.014.
Values may be sent and summed in bfloat16 or wider, within the bound.
A program may use at most 128 MiB of HBM per device.

v0:
```python
import jax
import jax.numpy as jnp
from jax import lax
from jax.sharding import PartitionSpec as P

KEY_DIM = 64
VAL_DIM = 128
BLOCK = 64


exact_numeric_mode = lax.Precision.HIGHEST
eps_value = 1e-06


def carried_in(part, axis, combine, identity, reverse):
    count = lax.axis_size(axis)
    place = lax.axis_index(axis)
    ahead = count - 1 - place if reverse else place
    gathered = jax.tree.map(lambda a: lax.all_gather(a, axis), part)
    state = jax.tree.map(lambda a, e: jnp.zeros_like(a) + jnp.asarray(e, a.dtype), part, identity)

    def one(lap, state):
        source = count - 1 - lap if reverse else lap
        return combine(
            state, jax.tree.map(lambda a: lax.dynamic_index_in_dim(a, source, 0, False), gathered)
        )

    return lax.fori_loop(0, ahead, one, state)


def chain_forward(earlier, later):
    return (earlier[0] * later[0], later[0][:, :, None] * earlier[1] + later[1])


def chain_backward(earlier, later):
    return (earlier[0] * later[0], later[1] + later[0][:, :, None] * earlier[1])


def carry_blocks(carried_state, inputs):
    decay_now, term_now = inputs
    return (decay_now[:, :, None] * carried_state + term_now, carried_state)


def body(
    hidden_state,
    norm_gain,
    route_ids,
    route_logits,
    cotangent,
    w_gate,
    w_up,
    w_down,
    w_out,
    query_rows,
    key_rows,
    value_rows,
    log_decay,
    head_gain,
):
    tok_count, model_width = hidden_state.shape
    head_count = head_gain.shape[0] // VAL_DIM
    block_count = tok_count // BLOCK
    shape_key = (block_count, BLOCK, head_count, KEY_DIM)
    shape_value = (block_count, BLOCK, head_count, VAL_DIM)
    query_f = query_rows.astype(jnp.float32).reshape(shape_key)
    key_f = key_rows.astype(jnp.float32).reshape(shape_key)
    value_f = value_rows.astype(jnp.float32).reshape(shape_value)
    cumulative_decay = jnp.cumsum(log_decay.reshape(shape_key), axis=1)
    decay_mid = cumulative_decay[:, BLOCK // 2 : BLOCK // 2 + 1]
    final_decay = cumulative_decay[:, BLOCK - 1 : BLOCK]
    query_in = query_f * jnp.exp(cumulative_decay - decay_mid)
    key_in = key_f * jnp.exp(decay_mid - cumulative_decay)
    key_end = key_f * jnp.exp(final_decay - cumulative_decay)
    query_start = query_f * jnp.exp(cumulative_decay)
    causal = (jnp.arange(BLOCK)[:, None] >= jnp.arange(BLOCK)[None, :])[None, None]
    last_logs = final_decay[:, 0]
    through = jnp.cumsum(last_logs, axis=0)
    total_log = through[-1]
    total_decay = jnp.exp(total_log)
    block_decay = jnp.exp(last_logs)
    block_kv = jnp.einsum("bshk,bshv->bhkv", key_end, value_f, precision=exact_numeric_mode)
    zero_state = jnp.zeros((head_count, KEY_DIM, VAL_DIM), jnp.float32)
    ones_decay = jnp.ones_like(total_log)
    local_end, local_start = lax.scan(carry_blocks, zero_state, (block_decay, block_kv))
    ahead = carried_in(
        (total_decay, local_end), "sp", chain_forward, (ones_decay, zero_state), False
    )
    state_in = ahead[1]
    block_states = local_start + jnp.exp(through - last_logs)[:, :, :, None] * state_in
    end_state = total_decay[:, :, None] * state_in + local_end
    scores = jnp.where(
        causal, jnp.einsum("bthk,bshk->bhts", query_in, key_in, precision=exact_numeric_mode), 0.0
    )
    head_out = jnp.einsum("bhts,bshv->bthv", scores, value_f, precision=exact_numeric_mode)
    head_out = head_out + jnp.einsum(
        "bthk,bhkv->bthv", query_start, block_states, precision=exact_numeric_mode
    )
    inv_rms = lax.rsqrt(jnp.mean(head_out * head_out, axis=-1, keepdims=True) + eps_value)
    normed = head_out * inv_rms
    gain_heads = head_gain.reshape(head_count, VAL_DIM)
    mixed_out = (normed * gain_heads).reshape(tok_count, head_count * VAL_DIM).astype(jnp.bfloat16)
    state_f = hidden_state.astype(jnp.float32)
    row_scale = lax.rsqrt(jnp.mean(state_f * state_f, axis=-1, keepdims=True) + eps_value)
    unit_rows = state_f * row_scale
    normed_in = (unit_rows * norm_gain).astype(jnp.bfloat16)
    route_weight = jax.nn.softmax(route_logits, axis=-1)
    cot_f = cotangent.astype(jnp.float32)
    slot_grads = (
        (route_weight[:, :, None] * cot_f[:, None, :])
        .astype(jnp.bfloat16)
        .reshape(2 * tok_count, model_width)
    )
    expert_count = lax.axis_size("sp")
    capacity = 4 * tok_count // expert_count
    flat_ids = route_ids.reshape(-1)
    one_hot = (flat_ids[:, None] == jnp.arange(expert_count, dtype=jnp.int32)[None, :]).astype(
        jnp.int32
    )
    slot_rank = jnp.sum((jnp.cumsum(one_hot, axis=0) - 1) * one_hot, axis=1)
    slot_of = flat_ids * capacity + slot_rank
    source = (
        jnp.full((expert_count * capacity,), 2 * tok_count, jnp.int32)
        .at[slot_of]
        .set(jnp.arange(2 * tok_count, dtype=jnp.int32))
    )
    token_of = jnp.where(source < 2 * tok_count, source // 2, tok_count)
    padded_in = jnp.concatenate([normed_in, jnp.zeros((1, model_width), jnp.bfloat16)], axis=0)
    padded_grad = jnp.concatenate([slot_grads, jnp.zeros((1, model_width), jnp.bfloat16)], axis=0)
    send_in = padded_in[token_of].reshape(expert_count, capacity, model_width)
    send_grad = padded_grad[source].reshape(expert_count, capacity, model_width)
    part_width = model_width // lax.axis_size("tp")
    feature_start = lax.axis_index("tp") * part_width
    part_in = lax.dynamic_slice_in_dim(send_in, feature_start, part_width, 2)
    part_grad = lax.dynamic_slice_in_dim(send_grad, feature_start, part_width, 2)
    part_in, part_grad = (
        lax.all_to_all(part_in, "sp", split_axis=0, concat_axis=0, tiled=True),
        lax.all_to_all(part_grad, "sp", split_axis=0, concat_axis=0, tiled=True),
    )
    got_in, got_grad = (
        lax.all_gather(part_in, "tp", axis=2, tiled=True),
        lax.all_gather(part_grad, "tp", axis=2, tiled=True),
    )
    rows_in = got_in.reshape(-1, model_width)
    rows_grad = got_grad.reshape(-1, model_width)
    gate_w = w_gate[0]
    up_w = w_up[0]
    down_w = w_down[0]
    gate_pre = jnp.dot(rows_in, gate_w, preferred_element_type=jnp.float32)
    up_pre = jnp.dot(rows_in, up_w, preferred_element_type=jnp.float32)
    gate_sig = jax.nn.sigmoid(gate_pre)
    silu_gate = gate_pre * gate_sig
    hidden_units = (silu_gate * up_pre).astype(jnp.bfloat16)
    grad_down = jnp.einsum("rf,rd->fd", hidden_units, rows_grad, preferred_element_type=jnp.float32)
    grad_hidden = jnp.einsum("rd,fd->rf", rows_grad, down_w, preferred_element_type=jnp.float32)
    grad_gate_pre = (grad_hidden * up_pre * gate_sig * (1.0 + gate_pre * (1.0 - gate_sig))).astype(
        jnp.bfloat16
    )
    grad_up_pre = (grad_hidden * silu_gate).astype(jnp.bfloat16)
    grad_gate_w = jnp.einsum(
        "rd,rf->df", rows_in, grad_gate_pre, preferred_element_type=jnp.float32
    )
    grad_up_w = jnp.einsum("rd,rf->df", rows_in, grad_up_pre, preferred_element_type=jnp.float32)
    partial_rows = jnp.einsum(
        "rf,df->rd", grad_gate_pre, gate_w, preferred_element_type=jnp.float32
    )
    partial_rows = partial_rows + jnp.einsum(
        "rf,df->rd", grad_up_pre, up_w, preferred_element_type=jnp.float32
    )
    partial_rows = partial_rows.reshape(expert_count, capacity, model_width)
    summed = lax.psum_scatter(
        partial_rows.astype(jnp.bfloat16), "tp", scatter_dimension=2, tiled=True
    )
    returned = lax.all_to_all(summed, "sp", split_axis=0, concat_axis=0, tiled=True)
    picked = returned.reshape(-1, part_width)[slot_of].reshape(tok_count, 2, part_width)
    picked = lax.all_gather(picked, "tp", axis=2, tiled=True)
    grad_normed = jnp.sum(picked.astype(jnp.float32), axis=1)
    grad_unit = grad_normed * norm_gain
    grad_state = row_scale * (
        grad_unit - unit_rows * jnp.mean(grad_unit * unit_rows, axis=-1, keepdims=True)
    )
    grad_mixed = (cot_f + grad_state).astype(jnp.bfloat16)
    grad_out_w = lax.psum_scatter(
        jnp.einsum("td,th->dh", grad_mixed, mixed_out, preferred_element_type=jnp.float32),
        "sp",
        scatter_dimension=0,
        tiled=True,
    )
    grad_mix = jnp.dot(grad_mixed, w_out, preferred_element_type=jnp.float32).astype(jnp.bfloat16)
    grad_mix = lax.optimization_barrier(grad_mix).astype(jnp.float32).reshape(shape_value)
    grad_scaled = grad_mix * gain_heads
    grad_out = inv_rms * (
        grad_scaled - normed * jnp.mean(grad_scaled * normed, axis=-1, keepdims=True)
    )
    block_adj = jnp.einsum("bthk,bthv->bhkv", query_start, grad_out, precision=exact_numeric_mode)
    local_adj, later_adj = lax.scan(
        carry_blocks, zero_state, (block_decay, block_adj), reverse=True
    )
    behind = carried_in(
        (total_decay, local_adj), "sp", chain_backward, (ones_decay, zero_state), True
    )
    adj_end = behind[1]
    block_adj_end = later_adj + jnp.exp(total_log - through)[:, :, :, None] * adj_end
    grad_dots = jnp.where(
        causal, jnp.einsum("bthv,bshv->bhts", grad_out, value_f, precision=exact_numeric_mode), 0.0
    )
    grad_query = jnp.exp(cumulative_decay - decay_mid) * jnp.einsum(
        "bhts,bshk->bthk", grad_dots, key_in, precision=exact_numeric_mode
    )
    grad_query = grad_query + jnp.exp(cumulative_decay) * jnp.einsum(
        "bthv,bhkv->bthk", grad_out, block_states, precision=exact_numeric_mode
    )
    grad_key = jnp.exp(decay_mid - cumulative_decay) * jnp.einsum(
        "bhts,bthk->bshk", grad_dots, query_in, precision=exact_numeric_mode
    )
    grad_key = grad_key + jnp.exp(final_decay - cumulative_decay) * jnp.einsum(
        "bhkv,bshv->bshk", block_adj_end, value_f, precision=exact_numeric_mode
    )
    grad_value = jnp.einsum("bhts,bthv->bshv", scores, grad_out, precision=exact_numeric_mode)
    grad_value = grad_value + jnp.einsum(
        "bshk,bhkv->bshv", key_end, block_adj_end, precision=exact_numeric_mode
    )
    log_terms = (query_f * grad_query - key_f * grad_key).reshape(tok_count, head_count * KEY_DIM)
    suffix = lax.cumsum(log_terms, axis=0, reverse=True)
    tail_term = jnp.sum(adj_end * end_state, axis=-1).reshape(1, head_count * KEY_DIM)
    grad_log = suffix + tail_term
    return (
        grad_gate_w.astype(jnp.bfloat16)[None],
        grad_up_w.astype(jnp.bfloat16)[None],
        grad_down.astype(jnp.bfloat16)[None],
        grad_out_w,
        grad_query.reshape(tok_count, -1).astype(jnp.bfloat16),
        grad_key.reshape(tok_count, -1).astype(jnp.bfloat16),
        grad_value.reshape(tok_count, -1).astype(jnp.bfloat16),
        grad_log,
    )


def solution(mesh):
    in_specs = (
        P("sp", None),
        P(),
        P("sp", None),
        P("sp", None),
        P("sp", None),
        P("sp", None, "tp"),
        P("sp", None, "tp"),
        P("sp", "tp", None),
        P(None, "tp"),
        P("sp", "tp"),
        P("sp", "tp"),
        P("sp", "tp"),
        P("sp", "tp"),
        P("tp"),
    )
    out_specs = (
        P("sp", None, "tp"),
        P("sp", None, "tp"),
        P("sp", "tp", None),
        P("sp", "tp"),
        P("sp", "tp"),
        P("sp", "tp"),
        P("sp", "tp"),
        P("sp", "tp"),
    )
    return jax.shard_map(body, mesh=mesh, in_specs=in_specs, out_specs=out_specs, check_vma=False)
```

profile of v0, /device:TPU:0, one launch (start us, length us, event | category | flops | bytes accessed | tf_op | source)
XLA Modules:
  0.0 271.8 jit_solution(8001065008882997877)
XLA Ops:
  7.2 0.8 broadcast_multiply_fusion.1
  8.0 0.8 copy.65
  9.1 1.2 fusion.30
  10.6 0.6 reduce-window.6
  11.6 1.4 scatter_custom_fusion
  13.0 1.2 fusion.24
  14.3 3.3 %gather_fusion = bf16[512,2048]{1,0:T(8,128)(2,1)} fusion(bf16[129,2048]{1,0:T(8,128)(2,1)S(1)} %concatenate.6, s32[1024]{0:T(1024)S(1)} %get-tuple-element.370), kind=kCustom, calls=%fused_computation | custom fusion | bytes 4196352 | tf_op jit(solution)/shard_map/gather | solution.py:129
  17.6 1.1 constant_dynamic-slice_fusion.1
  18.8 21.7 %all_to_all.15 = bf16[8,64,512]{2,1,0:T(8,128)(2,1)} all-to-all(bf16[8,64,512]{2,1,0:T(8,128)(2,1)S(1)} %constant_dynamic-slice_fusion.1), channel_id=1, replica_groups=mesh['sp'=8,'tp'=4] {'sp'}, dimensions={0} | all-to-all | bytes 1048576 | tf_op jit(solution)/shard_map/all_to_all | solution.py:136
  40.6 2.4 mul.303
  43.0 3.7 %mul.304 = f32[256,2048]{1,0:T(8,128)} reshape(f32[128,2,2048]{2,1,0:T(2,128)} %mul.303) | data formatting | bytes 4194304 | tf_op jit(solution)/shard_map/mul | solution.py:109
  47.0 2.1 multiply_convert_fusion
  49.2 3.3 %gather_fusion.1 = bf16[512,2048]{1,0:T(8,128)(2,1)} fusion(bf16[257,2048]{1,0:T(8,128)(2,1)S(1)} %concatenate.7, s32[1024]{0:T(1024)S(1)} %get-tuple-element.369), kind=kCustom, calls=%fused_computation.1 | custom fusion | bytes 4196352 | tf_op jit(solution)/shard_map/gather | solution.py:130
  52.5 1.1 constant_dynamic-slice_fusion
  53.6 17.4 %all_to_all.16 = bf16[8,64,512]{2,1,0:T(8,128)(2,1)} all-to-all(bf16[8,64,512]{2,1,0:T(8,128)(2,1)S(1)} %constant_dynamic-slice_fusion), channel_id=1, replica_groups=mesh['sp'=8,'tp'=4] {'sp'}, dimensions={0} | all-to-all | bytes 1048576 | tf_op jit(solution)/shard_map/all_to_all | solution.py:137
  71.1 3.9 %fusion.5 = f32[512,384]{1,0:T(8,128)} fusion(bf16[512,2048]{1,0:T(8,128)(2,1)} %bitcast.165, bf16[1,2048,384]{2,1,0:T(8,128)(2,1)S(1)} %copy-done), kind=kOutput, calls=%fused_computation.25 | convolution fusion | flops 805306368 | bytes 4456448 | tf_op jit(solution)/shard_map/dot_general | solution.py:148
  75.0 2.2 fusion.8
  77.1 15.6 %all-gather.8.cloned.1.call-done = bf16[8,64,2048]{2,1,0:T(8,128)(2,1)} async-done(((bf16[8,64,512]{2,1,0:T(8,128)(2,1)}), bf16[8,64,2048]{2,1,0:T(8,128)(2,1)}) %all-gather.8.cloned.1.call-update) | async-done | bytes 2097168 | tf_op jit(solution)/shard_map/all_gather | solution.py:141
  92.8 3.9 %multiply_convert_fusion.2 = (bf16[512,384]{1,0:T(8,128)(2,1)S(1)}, bf16[512,384]{1,0:T(8,128)(2,1)S(1)}) fusion(f32[512,384]{1,0:T(8,128)} %fusion.5, f32[512,384]{1,0:T(8,128)} %fusion.8, bf16[512,2048]{1,0:T(8,128)(2,1)} %bitcast.169, bf16[1,384,2048]{2,1,0:T(8,128)(2,1)} %param.29), kind=kOutput, calls=%fused_computation.64 | convolution fusion | flops 807862272 | bytes 6029312 | tf_op jit(solution)/shard_map/rd,fd->rf/dot_general | solution.py:154
  96.7 1.3 fusion.3
  98.0 2.7 add_convert_fusion
  100.7 0.8 copy-done.14
  102.1 20.5 %all_gather.30 = f32[8,2,64]{2,1,0:T(2,128)S(1)} all-gather(f32[1,2,64]{2,1,0:T(2,128)S(1)} %get-tuple-element.363), channel_id=1, replica_groups=mesh['sp'=8,'tp'=4] {'sp'}, dimensions={0}, use_global_device_ids=true | all-gather | bytes 4608 | tf_op jit(solution)/shard_map/all_gather | solution.py:19
  122.7 0.6 subtract_exponential_fusion.4
  123.9 31.5 %all-gather = f32[16,64,128]{2,1,0:T(8,128)S(1)} all-gather(f32[2,64,128]{2,1,0:T(8,128)S(1)} %get-tuple-element.269), channel_id=2, replica_groups=mesh['sp'=8,'tp'=4] {'sp'}, dimensions={0}, use_global_device_ids=true | all-gather | bytes 589824 | tf_op jit(solution)/shard_map/all_gather | solution.py:19
  155.4 3.7 %all-to-all-start.2 = ((bf16[8,64,512]{2,1,0:T(8,128)(2,1)}), bf16[8,64,512]{2,1,0:T(8,128)(2,1)S(1)}, u32[]{:S(2)}, u32[]{:S(2)}) async-start(bf16[8,64,512]{2,1,0:T(8,128)(2,1)} %reduce-scatter.3.cloned.1.call-done), calls=%async_computation.3 | async-start | bytes 1048576 | tf_op jit(solution)/shard_map/all_to_all | solution.py:173
  159.2 0.6 copy-done.16
  160.1 0.4 convolution_bitcast_fusion.4
  160.5 0.5 convolution_select_fusion.1
  161.0 8.2 %all-to-all-done.2 = bf16[8,64,512]{2,1,0:T(8,128)(2,1)S(1)} async-done(((bf16[8,64,512]{2,1,0:T(8,128)(2,1)}), bf16[8,64,512]{2,1,0:T(8,128)(2,1)S(1)}, u32[]{:S(2)}, u32[]{:S(2)}) %all-to-all-start.2) | async-done | bytes 524320 | tf_op jit(solution)/shard_map/all_to_all | solution.py:173
  169.3 1.2 gather_fusion.2
  170.4 0.8 reshape.200
  171.3 0.6 fusion.71
  172.2 0.6 add_rsqrt_fusion
  172.8 4.2 %fusion = bf16[1,2048,384]{2,1,0:T(8,128)(2,1)} fusion(bf16[512,2048]{1,0:T(8,128)(2,1)} %bitcast.166, bf16[512,384]{1,0:T(8,128)(2,1)} %copy-done.8), kind=kOutput, calls=%fused_computation.18 | convolution fusion | flops 806092800 | bytes 4063232 | tf_op jit(solution)/shard_map/rd,rf->df/dot_general | solution.py:159
  177.1 2.5 fusion.1
  179.5 2.2 fusion.2
  181.8 4.7 %all-gather.10.cloned.1.call-done = bf16[128,2,2048]{2,1,0:T(2,128)(2,1)} async-done(((bf16[128,2,512]{2,1,0:T(2,128)(2,1)}), bf16[128,2,2048]{2,1,0:T(2,128)(2,1)}) %all-gather.10.cloned.1.call-update) | async-done | bytes 1048592 | tf_op jit(solution)/shard_map/all_gather | solution.py:175
  186.5 4.2 %convert_reduce_fusion = f32[128,2048]{1,0:T(8,128)S(1)} fusion(bf16[128,2,2048]{2,1,0:T(2,128)(2,1)} %all-gather.10.cloned.1.call-done), kind=kLoop, calls=%fused_computation.21 | loop fusion | flops 786432 | bytes 2097152 | tf_op jit(solution)/shard_map/reduce_sum | solution.py:176
  190.7 0.3 fusion.25
  191.0 0.4 fusion.29
  191.4 0.5 copy-done.7
  192.3 0.9 multiply_reduce_fusion
  193.4 1.8 fusion.38
  196.0 32.7 %all-gather.1 = f32[16,64,128]{2,1,0:T(8,128)S(1)} all-gather(f32[2,64,128]{2,1,0:T(8,128)S(1)} %get-tuple-element.272), channel_id=3, replica_groups=mesh['sp'=8,'tp'=4] {'sp'}, dimensions={0}, use_global_device_ids=true | all-gather | bytes 589824 | tf_op jit(solution)/shard_map/all_gather | solution.py:19
  228.9 5.9 %while.57 = (s32[]{:T(128)}, f32[2,64,128]{2,1,0:T(8,128)S(1)}, s32[]{:T(128)}, f32[8,2,64,128]{3,2,1,0:T(8,128)S(1)}, f32[8,2,64]{2,1,0:T(2,128)}, /*index=5*/s32[]{:T(128)}, s32[]{:T(128)}, s32[]{:T(128)}, s32[]{:T(128)}) while((s32[]{:T(128)}, f32[2,64,128]{2,1,0:T(8,128)S(1)}, s32[]{:T(128)}, f32[8,2,64,128]{3,2,1,0:T(8,128)S(1)}, ...), condition=%wide.region_22.23_spmd, body=%wide.region_21.22_spmd.sunk | while | flops 32774 | bytes 198299 | solution.py:28
  228.9 0.7 dynamic-slice_bitcast_fusion.9
  229.7 0.7 dynamic-slice_bitcast_fusion.9
  230.5 0.7 dynamic-slice_bitcast_fusion.9
  231.3 0.7 dynamic-slice_bitcast_fusion.9
  232.2 0.7 dynamic-slice_bitcast_fusion.9
  233.0 0.7 dynamic-slice_bitcast_fusion.9
  233.8 0.7 dynamic-slice_bitcast_fusion.9
  235.1 0.4 fusion.19
  235.5 0.4 fusion.18
  236.0 0.3 multiply_subtract_fusion
  236.4 0.7 convert_element_type.101
  237.2 0.7 convert_element_type.103
  237.9 0.4 fusion.75
  238.4 0.5 fusion.23
  238.9 0.6 copy.120
  240.1 1.1 reduce_window_sum.48
  241.2 0.6 broadcast_add_fusion
  241.8 23.5 %reduce-scatter.5.cloned.1.call-done = f32[256,256]{1,0:T(8,128)} async-done(((f32[2048,256]{1,0:T(8,128)}), f32[256,256]{1,0:T(8,128)}) %reduce-scatter.5.cloned.1.call-update) | async-done | bytes 262160 | tf_op jit(solution)/shard_map/reduce_scatter | solution.py:182
  (169 shorter events, 7.1 us)
Async XLA Ops:
  7.2 63.9 %copy-start = (bf16[1,2048,384]{2,1,0:T(8,128)(2,1)S(1)}, bf16[1,2048,384]{2,1,0:T(8,128)(2,1)}, u32[]{:S(2)}) copy-start(bf16[1,2048,384]{2,1,0:T(8,128)(2,1)} %param.27) | copy-start | bytes 4718596
  7.2 63.9 %all-gather.6.cloned.1.call-start = ((), (), s32[]{:S(2)}) async-start(), calls=%async_computation.5 | async-start | bytes 2621440 | tf_op jit(solution)/shard_map/all_gather | solution.py:140
  10.3 4.0 %copy-start.30 = (f32[128]{0:T(128)}, f32[128]{0:T(128)S(1)}, u32[]{:S(2)}) copy-start(f32[128]{0:T(128)S(1)} %add_rsqrt_fusion.1) | copy-start | bytes 1540
  17.6 23.0 %copy-start.2 = (bf16[128,2048]{1,0:T(8,128)(2,1)S(1)}, bf16[128,2048]{1,0:T(8,128)(2,1)}, u32[]{:S(2)}) copy-start(bf16[128,2048]{1,0:T(8,128)(2,1)} %param.26) | copy-start | bytes 1572868
  40.5 52.2 %all-gather.8.cloned.1.call-start = ((), (), s32[]{:S(2)}) async-start(), calls=%async_computation.6 | async-start | bytes 2621440 | tf_op jit(solution)/shard_map/all_gather | solution.py:141
  43.0 3.7 %copy-start.29 = (f32[128,2]{0,1:T(2,128)S(1)}, f32[128,2]{0,1:T(2,128)}, u32[]{:S(2)}) copy-start(f32[128,2]{0,1:T(2,128)} %param.25) | copy-start | bytes 3076
  71.0 84.4 %reduce-scatter.3.cloned.1.call-start = ((), (), s32[]{:S(2)}) async-start(), calls=%async_computation.7 | async-start | bytes 2621440 | tf_op jit(solution)/shard_map/reduce_scatter | solution.py:170
  71.1 3.9 %copy-start.4 = (bf16[1,2048,384]{2,1,0:T(8,128)(2,1)S(1)}, bf16[1,2048,384]{2,1,0:T(8,128)(2,1)}, u32[]{:S(2)}) copy-start(bf16[1,2048,384]{2,1,0:T(8,128)(2,1)} %param.28) | copy-start | bytes 4718596
  71.1 3.9 %copy-start.35 = (bf16[8,64,2048]{2,1,0:T(8,128)(2,1)S(1)}, bf16[8,64,2048]{2,1,0:T(8,128)(2,1)}, u32[]{:S(2)}) copy-start(bf16[8,64,2048]{2,1,0:T(8,128)(2,1)} %all-gather.6.cloned.1.call-done) | copy-start | bytes 6291460
  96.6 1.3 copy-start.8
  96.7 1.3 copy-start.9
  100.6 0.8 copy-start.14
  100.6 1.0 copy-start.15
  100.6 1.0 copy-start.20
  102.1 21.4 %copy-start.27 = (f32[2,2,64]{2,1,0:T(2,128)}, f32[2,2,64]{2,1,0:T(2,128)S(1)}, u32[]{:S(2)}) copy-start(f32[2,2,64]{2,1,0:T(2,128)S(1)} %fusion.72) | copy-start | bytes 3076
  122.6 36.5 %copy-start.17 = (f32[2,2,64]{2,1,0:T(2,128)}, f32[2,2,64]{2,1,0:T(2,128)S(1)}, u32[]{:S(2)}) copy-start(f32[2,2,64]{2,1,0:T(2,128)S(1)} %get-tuple-element.358) | copy-start | bytes 3076
  123.2 36.8 %copy-start.25 = (f32[2,2,64]{2,1,0:T(2,128)}, f32[2,2,64]{2,1,0:T(2,128)S(1)}, u32[]{:S(2)}) copy-start(f32[2,2,64]{2,1,0:T(2,128)S(1)} %get-tuple-element.359) | copy-start | bytes 3076
  123.5 36.2 %copy-start.21 = (bf16[128,128]{1,0:T(8,128)(2,1)S(1)}, bf16[128,128]{1,0:T(8,128)(2,1)}, u32[]{:S(2)}) copy-start(bf16[128,128]{1,0:T(8,128)(2,1)} %param.31) | copy-start | bytes 98308
  123.9 37.2 %copy-start.5 = (f32[2,2,64,128]{3,2,1,0:T(8,128)}, f32[2,2,64,128]{3,2,1,0:T(8,128)S(1)}, u32[]{:S(2)}) copy-start(f32[2,2,64,128]{3,2,1,0:T(8,128)S(1)} %get-tuple-element.268) | copy-start | bytes 393220
  155.4 13.9 %all-to-all-start.2 = ((bf16[8,64,512]{2,1,0:T(8,128)(2,1)}), bf16[8,64,512]{2,1,0:T(8,128)(2,1)S(1)}, u32[]{:S(2)}, u32[]{:S(2)}) async-start(bf16[8,64,512]{2,1,0:T(8,128)(2,1)} %reduce-scatter.3.cloned.1.call-done), calls=%async_computation.3 | async-start | bytes 1048576 | tf_op jit(solution)/shard_map/all_to_all | solution.py:173
  159.1 27.4 %all-gather.10.cloned.1.call-start = ((), (), s32[]{:S(2)}) async-start(), calls=%async_computation.8 | async-start | bytes 1310720 | tf_op jit(solution)/shard_map/all_gather | solution.py:175
  159.2 0.6 copy-start.16
  160.1 11.2 %copy-start.12 = (pred[64,64]{1,0:T(8,128)(4,1)}, pred[64,64]{1,0:T(8,128)(4,1)S(1)}, u32[]{:S(2)}) copy-start(pred[64,64]{1,0:T(8,128)(4,1)S(1)} %iota_compare_fusion) | copy-start | bytes 12292
  160.1 11.3 %copy-start.28 = (f32[2,2,64]{2,1,0:T(2,128)S(1)}, f32[2,2,64]{2,1,0:T(2,128)}, u32[]{:S(2)}) copy-start(f32[2,2,64]{2,1,0:T(2,128)} %copy-done.27) | copy-start | bytes 3076
  171.3 94.0 %reduce-scatter.5.cloned.1.call-start = ((), (), s32[]{:S(2)}) async-start(), calls=%async_computation.9 | async-start | bytes 2359296 | tf_op jit(solution)/shard_map/reduce_scatter | solution.py:182
  172.8 4.2 %copy-start.10 = (bf16[512,384]{1,0:T(8,128)(2,1)S(1)}, bf16[512,384]{1,0:T(8,128)(2,1)}, u32[]{:S(2)}) copy-start(bf16[512,384]{1,0:T(8,128)(2,1)} %copy-done.9) | copy-start | bytes 1179652
  172.8 4.2 %copy-start.36 = (bf16[8,64,2048]{2,1,0:T(8,128)(2,1)S(1)}, bf16[8,64,2048]{2,1,0:T(8,128)(2,1)}, u32[]{:S(2)}) copy-start(bf16[8,64,2048]{2,1,0:T(8,128)(2,1)} %all-gather.6.cloned.1.call-done) | copy-start | bytes 6291460
  177.0 2.5 copy-start.37
  177.0 2.5 copy-start.38
  177.1 2.5 copy-start.39
  181.8 8.9 %copy-start.1 = (bf16[128,2048]{1,0:T(8,128)(2,1)S(1)}, bf16[128,2048]{1,0:T(8,128)(2,1)}, u32[]{:S(2)}) copy-start(bf16[128,2048]{1,0:T(8,128)(2,1)} %param.22) | copy-start | bytes 1572868
  181.8 8.9 %copy-start.11 = (f32[2048]{0:T(1024)S(1)}, f32[2048]{0:T(1024)}, u32[]{:S(2)}) copy-start(f32[2048]{0:T(1024)} %param.23) | copy-start | bytes 24580
  181.8 8.9 %copy-start.31 = (f32[128]{0:T(128)S(1)}, f32[128]{0:T(128)}, u32[]{:S(2)}) copy-start(f32[128]{0:T(128)} %copy-done.30) | copy-start | bytes 1540
  186.4 4.6 %copy-start.3 = (bf16[128,2048]{1,0:T(8,128)(2,1)S(1)}, bf16[128,2048]{1,0:T(8,128)(2,1)}, u32[]{:S(2)}) copy-start(bf16[128,2048]{1,0:T(8,128)(2,1)} %param.26) | copy-start | bytes 1572868
  186.4 4.6 %copy-start.32 = (f32[128]{0:T(128)S(1)}, f32[128]{0:T(128)}, u32[]{:S(2)}) copy-start(f32[128]{0:T(128)} %copy-done.30) | copy-start | bytes 1540
  190.7 1.2 copy-start.7
  191.9 1.3 copy-start.22
  191.9 1.3 copy-start.33
  195.3 33.4 %copy-start.13 = (pred[64,64]{1,0:T(8,128)(4,1)S(1)}, pred[64,64]{1,0:T(8,128)(4,1)}, u32[]{:S(2)}) copy-start(pred[64,64]{1,0:T(8,128)(4,1)} %copy-done.12) | copy-start | bytes 12292
  195.6 39.2 %copy-start.18 = (f32[2,2,64]{2,1,0:T(2,128)S(1)}, f32[2,2,64]{2,1,0:T(2,128)}, u32[]{:S(2)}) copy-start(f32[2,2,64]{2,1,0:T(2,128)} %copy-done.17) | copy-start | bytes 3076
  195.6 39.2 %copy-start.23 = (f32[2,2,64]{2,1,0:T(2,128)S(1)}, f32[2,2,64]{2,1,0:T(2,128)}, u32[]{:S(2)}) copy-start(f32[2,2,64]{2,1,0:T(2,128)} %get-tuple-element.361) | copy-start | bytes 3076
  195.6 39.5 %copy-start.6 = (f32[2,2,64,128]{3,2,1,0:T(8,128)S(1)}, f32[2,2,64,128]{3,2,1,0:T(8,128)}, u32[]{:S(2)}) copy-start(f32[2,2,64,128]{3,2,1,0:T(8,128)} %copy-done.5) | copy-start | bytes 393220
  195.9 39.2 %copy-start.26 = (f32[2,2,64]{2,1,0:T(2,128)S(1)}, f32[2,2,64]{2,1,0:T(2,128)}, u32[]{:S(2)}) copy-start(f32[2,2,64]{2,1,0:T(2,128)} %copy-done.25) | copy-start | bytes 3076
  234.8 3.6 %copy-start.19 = (f32[2,2,64]{2,1,0:T(2,128)S(1)}, f32[2,2,64]{2,1,0:T(2,128)}, u32[]{:S(2)}) copy-start(f32[2,2,64]{2,1,0:T(2,128)} %copy-done.17) | copy-start | bytes 3076
  234.8 3.6 %copy-start.24 = (f32[2,2,64]{2,1,0:T(2,128)S(1)}, f32[2,2,64]{2,1,0:T(2,128)}, u32[]{:S(2)}) copy-start(f32[2,2,64]{2,1,0:T(2,128)} %get-tuple-element.361) | copy-start | bytes 3076
  235.5 4.3 %copy-start.34 = (f32[2,64]{1,0:T(2,128)S(1)}, f32[2,64]{1,0:T(2,128)}, u32[]{:S(2)}) copy-start(f32[2,64]{1,0:T(2,128)} %fusion.71) | copy-start | bytes 1540
Sparse Core Ops, SparseCore 0:
  40.6 21.5 all-gather.5
  71.1 21.6 all-gather.7
  100.8 31.1 reduce-scatter.2
  171.4 15.0 all-gather.9
  195.4 69.8 reduce-scatter.4
where the time goes:
time: 273 us; the launch traced here: 272 us
  blocking collectives  124 us (45%)
  waiting for transfers between devices  52.1 us (19%)
  local copies, waits for them, and re-layouts  31.2 us (11%)
  matrix products  29.2 us (11%)
  other arithmetic  16.3 us (6%)
  between operations  14.6 us (5%)
  starting transfers between devices  3.88 us (1%)
    all_gather x3, blocking collectives, carried_in(): gathered = jax.tree.map(lambda a: lax.all_gather(a, axis), part)  84.7 us
    reduce_scatter x1, waiting for transfers between devices, body(): lax.psum_scatter(jnp.einsum('td,th->dh', grad_mixed, mixed_out, preferred...  23.5 us
    all_to_all x1, blocking collectives, body(): lax.all_to_all(part_in, 'sp', split_axis=0, concat_axis=0, tiled=True)  21.7 us
    all_to_all x1, blocking collectives, body(): lax.all_to_all(part_grad, 'sp', split_axis=0, concat_axis=0, tiled=True)  17.4 us
    all_gather x1, waiting for transfers between devices, body(): lax.all_gather(part_grad, 'tp', axis=2, tiled=True)  15.6 us
    all_to_all x1, waiting for transfers between devices, body(): lax.all_to_all(summed, 'sp', split_axis=0, concat_axis=0, tiled=True)  8.25 us
    mul x3, local copies, waits for them, and re-layouts, body(): route_weight[:, :, None] * cot_f[:, None, :]  6.23 us
  transfers between devices with their start and end apart: 6, of which 4 were waited for; matrix products, arithmetic and copies ran while one was open for 17% of the time, Pallas kernels for 0%

commit v1 on v0

--- a/solution.py
+++ b/solution.py
@@ -1,44 +1,494 @@
+import functools
 import jax
 import jax.numpy as jnp
 from jax import lax
+from jax.experimental import pallas as pl
+from jax.experimental.pallas import tpu as pltpu
 from jax.sharding import PartitionSpec as P
 
 KEY_DIM = 64
 VAL_DIM = 128
 BLOCK = 64
+MESH = pl.DeviceIdType.MESH
 
 
 exact_numeric_mode = lax.Precision.HIGHEST
 eps_value = 1e-06
 
 
-def carried_in(part, axis, combine, identity, reverse):
-    count = lax.axis_size(axis)
-    place = lax.axis_index(axis)
-    ahead = count - 1 - place if reverse else place
-    gathered = jax.tree.map(lambda a: lax.all_gather(a, axis), part)
-    state = jax.tree.map(lambda a, e: jnp.zeros_like(a) + jnp.asarray(e, a.dtype), part, identity)
-
-    def one(lap, state):
-        source = count - 1 - lap if reverse else lap
-        return combine(
-            state, jax.tree.map(lambda a: lax.dynamic_index_in_dim(a, source, 0, False), gathered)
+def remote(src, dst, send, recv, sp, tp):
+    return pltpu.make_async_remote_copy(
+        src_ref=src, dst_ref=dst, send_sem=send, recv_sem=recv, device_id=(sp, tp), device_id_type=MESH
+    )
+
+
+def each(start, stop, step):
+    lax.fori_loop(start, stop, lambda k, _: (step(k), 0)[1], 0)
+
+
+def greet(n, me, tp, others):
+    barrier = pltpu.get_barrier_semaphore()
+
+    def hello(k):
+        pl.semaphore_signal(
+            barrier, inc=1, device_id=(lax.rem(me + k, n), tp), device_id_type=MESH
         )
 
-    return lax.fori_loop(0, ahead, one, state)
-
-
-def chain_forward(earlier, later):
-    return (earlier[0] * later[0], later[0][:, :, None] * earlier[1] + later[1])
-
-
-def chain_backward(earlier, later):
-    return (earlier[0] * later[0], later[1] + later[0][:, :, None] * earlier[1])
+    if n > 1:
+        each(1, n, hello)
+    for sp, other in others:
+        pl.semaphore_signal(barrier, inc=1, device_id=(sp, other), device_id_type=MESH)
+    pl.semaphore_wait(barrier, n - 1 + len(others))
+
+
+class Carry:
+    def __init__(self, n, me, tp, reverse, first, held, sent, scan, send_sem, recv_sem):
+        self.n, self.me, self.tp, self.reverse = n, me, tp, reverse
+        self.first, self.held, self.sent, self.scan = first, held, sent, scan
+        self.send_sem, self.recv_sem = send_sem, recv_sem
+        self.rows = first.shape[0] - 8
+        self.scan[...] = jnp.zeros_like(self.scan)
+
+    def parts(self, step):
+        d = 1 << step
+        n, me = self.n, self.me
+        if self.reverse:
+            to, has_to, has_from = lax.rem(me - d + n, n), me >= d, me + d < n
+        else:
+            to, has_to, has_from = lax.rem(me + d, n), me + d < n, me >= d
+        src = self.first if step == 0 else self.sent.at[step - 1]
+        copy = remote(
+            src, self.held.at[step], self.send_sem.at[step], self.recv_sem.at[step], to, self.tp
+        )
+        return copy, has_to, has_from
+
+    def send(self, step):
+        copy, has_to, _ = self.parts(step)
+        pl.when(has_to)(lambda: copy.start())
+
+    def receive(self, step, last):
+        copy, _, has_from = self.parts(step)
+        rows = self.rows
+        now = self.first if step == 0 else self.sent.at[step - 1]
+
+        @pl.when(has_from)
+        def _():
+            copy.wait_recv()
+
+        if not last:
+
+            @pl.when(has_from)
+            def _():
+                other = self.held[step]
+                mine = now[...]
+                self.sent[step] = mine[rows : rows + 1] * other
+                self.sent[step, :rows] += mine[:rows]
+
+            @pl.when(jnp.logical_not(has_from))
+            def _():
+                self.sent[step] = now[...]
+
+        @pl.when(has_from)
+        def _():
+            other = self.held[step]
+            if step == 0:
+                self.scan[...] = other
+            else:
+                mine = self.scan[...]
+                self.scan[...] = mine[rows : rows + 1] * other
+                self.scan[:rows, :] += mine[:rows]
+
+    def finish(self, steps):
+        for step in range(steps):
+            copy, has_to, _ = self.parts(step)
+            pl.when(has_to)(lambda copy=copy: copy.wait_send())
+
+
+def steps_of(n):
+    return max(1, (n - 1).bit_length())
+
+
+def carry_scratch(n, shape):
+    steps = steps_of(n)
+    return [
+        pltpu.VMEM((steps,) + shape, jnp.float32),
+        pltpu.VMEM((steps,) + shape, jnp.float32),
+        pltpu.SemaphoreType.DMA((steps,)),
+        pltpu.SemaphoreType.DMA((steps,)),
+    ]
+
+
+def tp_pair(tp):
+    return tp + 1 - 2 * lax.rem(tp, 2), lax.rem(tp + 2, 4)
+
+
+def dispatch_kernel(
+    n,
+    a_ref,
+    b_ref,
+    state_ref,
+    a_out,
+    b_out,
+    scan_out,
+    held,
+    sent,
+    carry_send,
+    carry_recv,
+    local_sem,
+    send_sem,
+    recv_sem,
+    pair_send,
+    pair_recv,
+    twin_send,
+    twin_recv,
+):
+    me, tp = lax.axis_index("sp"), lax.axis_index("tp")
+    pair, twin = tp_pair(tp)
+    width = a_ref.shape[2]
+    greet(n, me, tp, [(me, pair), (me, twin)])
+    steps = steps_of(n)
+    carry = Carry(n, me, tp, False, state_ref, held, sent, scan_out, carry_send, carry_recv)
+    ins, outs = (a_ref, b_ref), (a_out, b_out)
+
+    def lanes(t):
+        return pl.ds(pl.multiple_of(t * width, 128), width)
+
+    def exchange(j, k):
+        to = lax.rem(me + k, n)
+        return remote(
+            ins[j].at[to],
+            outs[j].at[me, :, lanes(tp)],
+            send_sem.at[j, k],
+            recv_sem.at[j, k],
+            to,
+            tp,
+        )
+
+    def own(j):
+        return pltpu.make_async_copy(
+            ins[j].at[me], outs[j].at[me, :, lanes(tp)], local_sem.at[j]
+        )
+
+    def forward(j, k, kind):
+        block = lax.rem(me - k + n, n)
+        if kind == 0:
+            piece = outs[j].at[block, :, lanes(tp)]
+            return remote(
+                piece, piece, twin_send.at[j, k], twin_recv.at[j, k], me, twin
+            )
+        piece = outs[j].at[block, :, lanes(tp if kind == 1 else twin)]
+        return remote(
+            piece, piece, pair_send.at[j, kind - 1, k], pair_recv.at[j, kind - 1, k], me, pair
+        )
+
+    def spread(j, k):
+        exchange(j, k).wait_recv()
+        forward(j, k, 0).start()
+        forward(j, k, 1).start()
+
+    def begin(j):
+        own(j).start()
+        each(1, n, lambda k: exchange(j, k).start())
+        own(j).wait()
+        forward(j, 0, 0).start()
+        forward(j, 0, 1).start()
+
+    def twin_done(j, k):
+        block = lax.rem(me - k + n, n)
+        forward(j, k, 0).wait_recv()
+        forward(j, k, 2).start()
+
+    half = n // 2
+    carry.send(0)
+    begin(0)
+    carry.receive(0, steps == 1)
+    if steps > 1:
+        carry.send(1)
+    each(1, half, lambda k: spread(0, k))
+    begin(1)
+    each(half, n, lambda k: spread(0, k))
+    for step in range(1, steps):
+        carry.receive(step, step == steps - 1)
+        if step + 1 < steps:
+            carry.send(step + 1)
+    each(1, half, lambda k: spread(1, k))
+    each(0, n, lambda k: twin_done(0, k))
+    each(half, n, lambda k: spread(1, k))
+    each(0, n, lambda k: twin_done(1, k))
+    carry.finish(steps)
+    for j in range(2):
+        each(1, n, lambda k: exchange(j, k).wait_send())
+
+        def finish(k):
+            forward(j, k, 0).wait_send()
+            for kind in (1, 2):
+                forward(j, k, kind).wait()
+
+        each(0, n, finish)
+
+
+def vmem(count):
+    return [pl.BlockSpec(memory_space=pltpu.VMEM)] * count
+
+
+def dispatch(n, part_in, part_grad, packed):
+    count, cap, width = part_in.shape
+    full = jax.ShapeDtypeStruct((count, cap, 4 * width), part_in.dtype)
+    dma = pltpu.SemaphoreType.DMA
+    return pl.pallas_call(
+        functools.partial(dispatch_kernel, n),
+        out_shape=[full, full, jax.ShapeDtypeStruct(packed.shape, jnp.float32)],
+        in_specs=vmem(3),
+        out_specs=vmem(3),
+        scratch_shapes=carry_scratch(n, packed.shape)
+        + [
+            dma((2,)),
+            dma((2, n)),
+            dma((2, n)),
+            dma((2, 2, n)),
+            dma((2, 2, n)),
+            dma((2, n)),
+            dma((2, n)),
+        ],
+        compiler_params=pltpu.CompilerParams(
+            collective_id=0, has_side_effects=True, vmem_limit_bytes=40 << 20
+        ),
+        name="dispatch",
+    )(part_in, part_grad, packed)
+
+
+def return_kernel(
+    n,
+    part_ref,
+    mix_ref,
+    back_out,
+    mix_out,
+    near,
+    far_sum,
+    far,
+    total,
+    local_sem,
+    near_send,
+    near_recv,
+    far_send,
+    far_recv,
+    send_sem,
+    recv_sem,
+    mix_send,
+    mix_recv,
+):
+    me, tp = lax.axis_index("sp"), lax.axis_index("tp")
+    pair, twin = tp_pair(tp)
+    pair_twin = lax.rem(pair + 2, 4)
+    width = back_out.shape[2]
+    greet(n, me, tp, [(me, pair), (me, twin)])
+
+    def lanes(t):
+        return pl.ds(pl.multiple_of(t * width, 128), width)
+
+    def to_pair(kind, k):
+        block = lax.rem(me + k, n)
+        return remote(
+            part_ref.at[block, :, lanes(pair if kind == 0 else pair_twin)],
+            near.at[kind, block],
+            near_send.at[kind, k],
+            near_recv.at[kind, k],
+            me,
+            pair,
+        )
+
+    def to_twin(k):
+        block = lax.rem(me + k, n)
+        return remote(far_sum.at[block], far.at[block], far_send.at[k], far_recv.at[k], me, twin)
+
+    def to_owner(k):
+        block = lax.rem(me + k, n)
+        return remote(total.at[block], back_out.at[me], send_sem.at[k], recv_sem.at[k], block, tp)
+
+    def mixed(k):
+        to = lax.rem(me + k, n)
+        return remote(mix_ref, mix_out.at[me], mix_send.at[k], mix_recv.at[k], to, tp)
+
+    each(1, n + 1, lambda k: to_pair(1, lax.rem(k, n)).start())
+    each(1, n + 1, lambda k: to_pair(0, lax.rem(k, n)).start())
+    each(1, n, lambda k: mixed(k).start())
+    own_mix = pltpu.make_async_copy(mix_ref, mix_out.at[me], local_sem.at[0])
+    own_mix.start()
+
+    def reduce_pair(i):
+        k = lax.rem(i, n)
+        block = lax.rem(me + k, n)
+        to_pair(1, k).wait_recv()
+        mine = part_ref[block, :, lanes(twin)].astype(jnp.float32)
+        far_sum[block] = (mine + near[1, block].astype(jnp.float32)).astype(jnp.bfloat16)
+        pl.when(i > 1)(lambda: to_twin(i - 1).start())
+
+    each(1, n + 1, reduce_pair)
+    to_twin(0).start()
+
+    def reduce_all(i):
+        k = lax.rem(i, n)
+        block = lax.rem(me + k, n)
+        to_pair(0, k).wait_recv()
+        to_twin(k).wait_recv()
+        mine = part_ref[block, :, lanes(tp)].astype(jnp.float32)
+        mine = mine + near[0, block].astype(jnp.float32) + far[block].astype(jnp.float32)
+        total[block] = mine.astype(jnp.bfloat16)
+        pl.when(i > 1)(lambda: to_owner(i - 1).start())
+
+    each(1, n + 1, reduce_all)
+    back_out[me] = total[me]
+    own_mix.wait()
+
+    def finish(k):
+        for kind in (0, 1):
+            to_pair(kind, k).wait_send()
+        to_twin(k).wait_send()
+
+    each(0, n, finish)
+
+    def finish_far(k):
+        to_owner(k).wait()
+        mixed(k).wait()
+
+    each(1, n, finish_far)
+
+
+def give_back(n, partial_rows, mixed_out):
+    count, cap, model_width = partial_rows.shape
+    width = model_width // 4
+    dma = pltpu.SemaphoreType.DMA
+    block = (count, cap, width)
+    return pl.pallas_call(
+        functools.partial(return_kernel, n),
+        out_shape=[
+            jax.ShapeDtypeStruct(block, jnp.bfloat16),
+            jax.ShapeDtypeStruct((n,) + mixed_out.shape, jnp.bfloat16),
+        ],
+        in_specs=vmem(2),
+        out_specs=vmem(2),
+        scratch_shapes=[
+            pltpu.VMEM((2,) + block, jnp.bfloat16),
+            pltpu.VMEM(block, jnp.bfloat16),
+            pltpu.VMEM(block, jnp.bfloat16),
+            pltpu.VMEM(block, jnp.bfloat16),
+            dma((1,)),
+            dma((2, n)),
+            dma((2, n)),
+            dma((n,)),
+            dma((n,)),
+            dma((n,)),
+            dma((n,)),
+            dma((n,)),
+            dma((n,)),
+        ],
+        compiler_params=pltpu.CompilerParams(
+            collective_id=1, has_side_effects=True, vmem_limit_bytes=40 << 20
+        ),
+        name="give_back",
+    )(partial_rows, mixed_out)
+
+
+def features_kernel(x_ref, out_ref, local_sem, send_sem, recv_sem):
+    me, tp = lax.axis_index("sp"), lax.axis_index("tp")
+    pair, twin = tp_pair(tp)
+    greet(1, me, tp, [(me, pair), (me, twin)])
+    own = pltpu.make_async_copy(x_ref, out_ref.at[tp], local_sem.at[0])
+    own.start()
+    copies = [
+        remote(x_ref, out_ref.at[tp], send_sem.at[0], recv_sem.at[0], me, twin),
+        remote(x_ref, out_ref.at[tp], send_sem.at[1], recv_sem.at[1], me, pair),
+        remote(out_ref.at[twin], out_ref.at[twin], send_sem.at[2], recv_sem.at[2], me, pair),
+    ]
+    copies[0].start()
+    copies[1].start()
+    copies[0].wait_recv()
+    copies[2].start()
+    copies[1].wait()
+    copies[2].wait()
+    copies[0].wait_send()
+    own.wait()
+
+
+def all_features(x):
+    dma = pltpu.SemaphoreType.DMA
+    return pl.pallas_call(
+        features_kernel,
+        out_shape=jax.ShapeDtypeStruct((4,) + x.shape, x.dtype),
+        in_specs=vmem(1),
+        out_specs=pl.BlockSpec(memory_space=pltpu.VMEM),
+        scratch_shapes=[dma((1,)), dma((3,)), dma((3,))],
+        compiler_params=pltpu.CompilerParams(collective_id=2, has_side_effects=True),
+        name="all_features",
+    )(x)
+
+
+def last_kernel(
+    n, rows_ref, state_ref, rows_out, scan_out, held, sent, carry_send, carry_recv, local_sem, send_sem, recv_sem
+):
+    me, tp = lax.axis_index("sp"), lax.axis_index("tp")
+    greet(n, me, tp, [])
+    steps = steps_of(n)
+    carry = Carry(n, me, tp, True, state_ref, held, sent, scan_out, carry_send, carry_recv)
+
+    def exchange(k):
+        to = lax.rem(me + k, n)
+        return remote(rows_ref.at[to], rows_out.at[me], send_sem.at[k], recv_sem.at[k], to, tp)
+
+    own = pltpu.make_async_copy(rows_ref.at[me], rows_out.at[me], local_sem.at[0])
+    carry.send(0)
+    own.start()
+    cuts = [1 + (n - 1) * i // steps for i in range(steps + 1)]
+    for step in range(steps):
+        each(cuts[step], cuts[step + 1], lambda k: exchange(k).start())
+        carry.receive(step, step == steps - 1)
+        if step + 1 < steps:
+            carry.send(step + 1)
+    carry.finish(steps)
+    own.wait()
+    each(1, n, lambda k: exchange(k).wait())
+
+
+def last_exchange(n, rows, packed):
+    dma = pltpu.SemaphoreType.DMA
+    return pl.pallas_call(
+        functools.partial(last_kernel, n),
+        out_shape=[
+            jax.ShapeDtypeStruct(rows.shape, rows.dtype),
+            jax.ShapeDtypeStruct(packed.shape, jnp.float32),
+        ],
+        in_specs=vmem(2),
+        out_specs=vmem(2),
+        scratch_shapes=carry_scratch(n, packed.shape) + [dma((1,)), dma((n,)), dma((n,))],
+        compiler_params=pltpu.CompilerParams(
+            collective_id=3, has_side_effects=True, vmem_limit_bytes=40 << 20
+        ),
+        name="last_exchange",
+    )(rows, packed)
+
+
+def pack_state(state, decay):
+    heads, keys, values = state.shape
+    rows = state.transpose(2, 0, 1).reshape(values, heads * keys)
+    return jnp.concatenate([rows, jnp.broadcast_to(decay.reshape(1, -1), (8, heads * keys))], axis=0)
+
+
+def unpack_state(packed, heads):
+    rows = packed[:-8]
+    return rows.reshape(rows.shape[0], heads, -1).transpose(1, 2, 0)
 
 
 def carry_blocks(carried_state, inputs):
     decay_now, term_now = inputs
     return (decay_now[:, :, None] * carried_state + term_now, carried_state)
+
+
+def block_scan(decays, terms, state, reverse):
+    count = decays.shape[0]
+    starts = [None] * count
+    for i in reversed(range(count)) if reverse else range(count):
+        state, starts[i] = carry_blocks(state, (decays[i], terms[i]))
+    return state, jnp.stack(starts)
 
 
 def body(
@@ -81,11 +531,38 @@
     block_kv = jnp.einsum("bshk,bshv->bhkv", key_end, value_f, precision=exact_numeric_mode)
     zero_state = jnp.zeros((head_count, KEY_DIM, VAL_DIM), jnp.float32)
     ones_decay = jnp.ones_like(total_log)
-    local_end, local_start = lax.scan(carry_blocks, zero_state, (block_decay, block_kv))
-    ahead = carried_in(
-        (total_decay, local_end), "sp", chain_forward, (ones_decay, zero_state), False
-    )
-    state_in = ahead[1]
+    local_end, local_start = block_scan(block_decay, block_kv, zero_state, False)
+    sp_count = lax.axis_size("sp")
+    state_f = hidden_state.astype(jnp.float32)
+    row_scale = lax.rsqrt(jnp.mean(state_f * state_f, axis=-1, keepdims=True) + eps_value)
+    part_width = model_width // lax.axis_size("tp")
+    feature_start = lax.axis_index("tp") * part_width
+    hidden_part = lax.dynamic_slice_in_dim(hidden_state, feature_start, part_width, 1)
+    gain_part = lax.dynamic_slice_in_dim(norm_gain, feature_start, part_width, 0)
+    cot_part = lax.dynamic_slice_in_dim(cotangent, feature_start, part_width, 1)
+    normed_part = (hidden_part.astype(jnp.float32) * row_scale * gain_part).astype(jnp.bfloat16)
+    route_weight = jax.nn.softmax(route_logits, axis=-1)
+    expert_count = sp_count
+    capacity = 4 * tok_count // expert_count
+    named = route_ids[:, :, None] == jnp.arange(expert_count, dtype=jnp.int32)[None, None, :]
+    names = jnp.any(named, axis=1)
+    weight_of = jnp.sum(jnp.where(named, route_weight[:, :, None], 0.0), axis=1)
+    before = (jnp.arange(tok_count)[:, None] > jnp.arange(tok_count)[None, :]).astype(jnp.bfloat16)
+    rank = jnp.dot(before, names.astype(jnp.bfloat16), preferred_element_type=jnp.float32)
+    place = jnp.where(names, rank, -1.0).T
+    filled = place[:, None, :] == jnp.arange(capacity, dtype=jnp.float32)[None, :, None]
+    slot_weight = jnp.sum(jnp.where(filled, weight_of.T[:, None, :], 0.0), axis=2)
+    pick = filled.astype(jnp.bfloat16).reshape(expert_count * capacity, tok_count)
+    send_in = jnp.dot(pick, normed_part, preferred_element_type=jnp.float32).astype(jnp.bfloat16)
+    send_grad = jnp.dot(pick, cot_part, preferred_element_type=jnp.float32)
+    send_grad = (send_grad * slot_weight.reshape(-1, 1)).astype(jnp.bfloat16)
+    got_in, got_grad, scanned = dispatch(
+        sp_count,
+        send_in.reshape(expert_count, capacity, part_width),
+        send_grad.reshape(expert_count, capacity, part_width),
+        pack_state(local_end, total_decay),
+    )
+    state_in = unpack_state(scanned, head_count)
     block_states = local_start + jnp.exp(through - last_logs)[:, :, :, None] * state_in
     end_state = total_decay[:, :, None] * state_in + local_end
     scores = jnp.where(
@@ -99,47 +576,8 @@
     normed = head_out * inv_rms
     gain_heads = head_gain.reshape(head_count, VAL_DIM)
     mixed_out = (normed * gain_heads).reshape(tok_count, head_count * VAL_DIM).astype(jnp.bfloat16)
-    state_f = hidden_state.astype(jnp.float32)
-    row_scale = lax.rsqrt(jnp.mean(state_f * state_f, axis=-1, keepdims=True) + eps_value)
     unit_rows = state_f * row_scale
-    normed_in = (unit_rows * norm_gain).astype(jnp.bfloat16)
-    route_weight = jax.nn.softmax(route_logits, axis=-1)
     cot_f = cotangent.astype(jnp.float32)
-    slot_grads = (
-        (route_weight[:, :, None] * cot_f[:, None, :])
-        .astype(jnp.bfloat16)
-        .reshape(2 * tok_count, model_width)
-    )
-    expert_count = lax.axis_size("sp")
-    capacity = 4 * tok_count // expert_count
-    flat_ids = route_ids.reshape(-1)
-    one_hot = (flat_ids[:, None] == jnp.arange(expert_count, dtype=jnp.int32)[None, :]).astype(
-        jnp.int32
-    )
-    slot_rank = jnp.sum((jnp.cumsum(one_hot, axis=0) - 1) * one_hot, axis=1)
-    slot_of = flat_ids * capacity + slot_rank
-    source = (
-        jnp.full((expert_count * capacity,), 2 * tok_count, jnp.int32)
-        .at[slot_of]
-        .set(jnp.arange(2 * tok_count, dtype=jnp.int32))
-    )
-    token_of = jnp.where(source < 2 * tok_count, source // 2, tok_count)
-    padded_in = jnp.concatenate([normed_in, jnp.zeros((1, model_width), jnp.bfloat16)], axis=0)
-    padded_grad = jnp.concatenate([slot_grads, jnp.zeros((1, model_width), jnp.bfloat16)], axis=0)
-    send_in = padded_in[token_of].reshape(expert_count, capacity, model_width)
-    send_grad = padded_grad[source].reshape(expert_count, capacity, model_width)
-    part_width = model_width // lax.axis_size("tp")
-    feature_start = lax.axis_index("tp") * part_width
-    part_in = lax.dynamic_slice_in_dim(send_in, feature_start, part_width, 2)
-    part_grad = lax.dynamic_slice_in_dim(send_grad, feature_start, part_width, 2)
-    part_in, part_grad = (
-        lax.all_to_all(part_in, "sp", split_axis=0, concat_axis=0, tiled=True),
-        lax.all_to_all(part_grad, "sp", split_axis=0, concat_axis=0, tiled=True),
-    )
-    got_in, got_grad = (
-        lax.all_gather(part_in, "tp", axis=2, tiled=True),
-        lax.all_gather(part_grad, "tp", axis=2, tiled=True),
-    )
     rows_in = got_in.reshape(-1, model_width)
     rows_grad = got_grad.reshape(-1, model_width)
     gate_w = w_gate[0]
@@ -167,24 +605,20 @@
         "rf,df->rd", grad_up_pre, up_w, preferred_element_type=jnp.float32
     )
     partial_rows = partial_rows.reshape(expert_count, capacity, model_width)
-    summed = lax.psum_scatter(
-        partial_rows.astype(jnp.bfloat16), "tp", scatter_dimension=2, tiled=True
-    )
-    returned = lax.all_to_all(summed, "sp", split_axis=0, concat_axis=0, tiled=True)
-    picked = returned.reshape(-1, part_width)[slot_of].reshape(tok_count, 2, part_width)
-    picked = lax.all_gather(picked, "tp", axis=2, tiled=True)
-    grad_normed = jnp.sum(picked.astype(jnp.float32), axis=1)
+    returned, mixed_all = give_back(sp_count, partial_rows.astype(jnp.bfloat16), mixed_out)
+    summed = lax.dot_general(
+        pick,
+        returned.reshape(-1, part_width),
+        (((0,), (0,)), ((), ())),
+        preferred_element_type=jnp.float32,
+    )
+    grad_normed = all_features(summed.astype(jnp.bfloat16)).astype(jnp.float32)
+    grad_normed = grad_normed.transpose(1, 0, 2).reshape(tok_count, model_width)
     grad_unit = grad_normed * norm_gain
     grad_state = row_scale * (
         grad_unit - unit_rows * jnp.mean(grad_unit * unit_rows, axis=-1, keepdims=True)
     )
     grad_mixed = (cot_f + grad_state).astype(jnp.bfloat16)
-    grad_out_w = lax.psum_scatter(
-        jnp.einsum("td,th->dh", grad_mixed, mixed_out, preferred_element_type=jnp.float32),
-        "sp",
-        scatter_dimension=0,
-        tiled=True,
-    )
     grad_mix = jnp.dot(grad_mixed, w_out, preferred_element_type=jnp.float32).astype(jnp.bfloat16)
     grad_mix = lax.optimization_barrier(grad_mix).astype(jnp.float32).reshape(shape_value)
     grad_scaled = grad_mix * gain_heads
@@ -192,13 +626,11 @@
         grad_scaled - normed * jnp.mean(grad_scaled * normed, axis=-1, keepdims=True)
     )
     block_adj = jnp.einsum("bthk,bthv->bhkv", query_start, grad_out, precision=exact_numeric_mode)
-    local_adj, later_adj = lax.scan(
-        carry_blocks, zero_state, (block_decay, block_adj), reverse=True
-    )
-    behind = carried_in(
-        (total_decay, local_adj), "sp", chain_backward, (ones_decay, zero_state), True
-    )
-    adj_end = behind[1]
+    local_adj, later_adj = block_scan(block_decay, block_adj, zero_state, True)
+    mixed_parts = grad_mixed.reshape(tok_count, sp_count, -1).transpose(1, 0, 2)
+    got_mixed, behind = last_exchange(sp_count, mixed_parts, pack_state(local_adj, total_decay))
+    grad_out_w = jnp.einsum("ntd,nth->dh", got_mixed, mixed_all, preferred_element_type=jnp.float32)
+    adj_end = unpack_state(behind, head_count)
     block_adj_end = later_adj + jnp.exp(total_log - through)[:, :, :, None] * adj_end
     grad_dots = jnp.where(
         causal, jnp.einsum("bthv,bshv->bhts", grad_out, value_f, precision=exact_numeric_mode), 0.0

time: 273 us -> 160 us (0.59)
  blocking collectives: 124 us -> 0 us
  Pallas kernels: 0 us -> 104 us
  waiting for transfers between devices: 52.1 us -> 0 us
  local copies, waits for them, and re-layouts: 31.2 us -> 12.8 us
  between operations: 14.6 us -> 1.59 us
  starting transfers between devices: 3.88 us -> 0 us
    pallas_call x0 -> x4, Pallas kernels: none -> 104 us  [the longest x1 37.1 us: dispatch(): pl.pallas_call(functools.partial(dispatch_kernel, n), out_shape=[full, fu...]
    all_gather x3 -> x0, blocking collectives: 84.7 us -> none  [carried_in(): gathered = jax.tree.map(lambda a: lax.all_gather(a, axis), part)]
    all_to_all x2 -> x0, blocking collectives: 39.1 us -> none  [the longest x1 21.7 us: body(): lax.all_to_all(part_in, 'sp', split_axis=0, concat_axis=0, tiled=True)]
    reduce_scatter x2 -> x0, waiting for transfers between devices: 23.5 us -> none  [the longest x1 23.5 us: body(): lax.psum_scatter(jnp.einsum('td,th->dh', grad_mixed, mixed_out, preferred...]
    all_gather x3 -> x0, waiting for transfers between devices: 20.3 us -> none  [the longest x1 15.6 us: body(): lax.all_gather(part_grad, 'tp', axis=2, tiled=True)]
    mul x12 -> x1, local copies, waits for them, and re-layouts: 11.3 us -> 0.08 us  [body(): send_grad = (send_grad * slot_weight.reshape(-1, 1)).astype(jnp.bfloat16)]
    all_to_all x1 -> x0, waiting for transfers between devices: 8.25 us -> none  [body(): lax.all_to_all(summed, 'sp', split_axis=0, concat_axis=0, tiled=True)]
    gather x3 -> x0, local copies, waits for them, and re-layouts: 7.79 us -> none  [the longest x1 3.32 us: body(): send_grad = padded_grad[source].reshape(expert_count, capacity, model_width)]
  transfers between devices with their start and end apart: 6 -> 0, of which waited for: 4 -> 0; matrix products, arithmetic and copies ran while one was open for 17% -> 0% of each run, Pallas kernels for 0% -> 0%
where the time goes in v1:
time: 160 us; the launch traced here: 159 us
  Pallas kernels  104 us (65%)
  matrix products  27.1 us (17%)
  other arithmetic  13.7 us (9%)
  local copies, waits for them, and re-layouts  12.8 us (8%)
    pallas_call x1, Pallas kernels, dispatch(): pl.pallas_call(functools.partial(dispatch_kernel, n), out_shape=[full, fu...  37.1 us
    pallas_call x1, Pallas kernels, give_back(): pl.pallas_call(functools.partial(return_kernel, n), out_shape=[jax.ShapeD...  34.8 us
    pallas_call x1, Pallas kernels, last_exchange(): pl.pallas_call(functools.partial(last_kernel, n), out_shape=[jax.ShapeDty...  23.5 us
    pallas_call x1, Pallas kernels, all_features(): pl.pallas_call(features_kernel, out_shape=jax.ShapeDtypeStruct((4,) + x.s...  8.4 us
    unnamed x94, local copies, waits for them, and re-layouts  5.13 us

profile of v1, /device:TPU:0, one launch (start us, length us, event | category | flops | bytes accessed | tf_op | source)
XLA Modules:
  0.0 159.0 jit_solution(8872139940216908233)
XLA Ops:
  0.8 0.8 fusion.67
  1.6 0.1 convolution_select_fusion.2
  1.7 0.2 bitcast_compare_fusion
  1.9 0.8 dynamic_slice.10
  2.6 1.3 copy.79
  4.0 0.3 fusion.30
  4.3 0.5 copy-done.2
  4.8 1.3 convolution_convert_fusion.3
  6.2 0.1 select_reduce_fusion
  6.4 1.2 fusion.12
  7.6 0.1 reshape.170
  8.0 0.1 reshape.189
  8.4 0.3 fusion.63
  8.6 0.6 subtract_exponential_fusion.4
  9.2 0.5 broadcast_multiply_fusion.1
  9.8 0.6 slice_bitcast_fusion.4
  10.5 0.4 copy-done.38
  11.0 37.1 %dispatch.1 = (bf16[8,64,2048]{2,1,0:T(8,128)(2,1)S(1)}, bf16[8,64,2048]{2,1,0:T(8,128)(2,1)S(1)}, f32[136,128]{1,0:T(8,128)S(1)}) custom-call(bf16[8,64,512]{2,1,0:T(8,128)(2,1)S(1)} %bitcast.171, bf16[8,64,512]{2,1,0:T(8,128)(2,1)S(1)} %bitcast.172, f32[136,128]{1,0:T(8,128)S(1)} %pad_maximum_fusion.1.state_ref), custom_call_target="tpu_custom_call" | custom-call | tf_op jit(solution)/shard_map/dispatch/pallas_call | solution.py:238
  48.2 1.2 fusion.5
  49.4 0.1 copy-done.9
  49.6 1.2 fusion.8
  50.8 0.2 copy-done.44
  51.0 1.4 multiply_convert_fusion.1
  52.4 2.4 %fusion = bf16[1,2048,384]{2,1,0:T(8,128)(2,1)} fusion(bf16[512,2048]{1,0:T(8,128)(2,1)S(1)} %bitcast.179, bf16[512,384]{1,0:T(8,128)(2,1)S(1)} %get-tuple-element.23), kind=kOutput, calls=%fused_computation.4 | convolution fusion | flops 806092800 | bytes 4063232 | tf_op jit(solution)/shard_map/rd,rf->df/dot_general | solution.py:597
  54.8 2.4 %fusion.1 = bf16[1,2048,384]{2,1,0:T(8,128)(2,1)} fusion(bf16[512,2048]{1,0:T(8,128)(2,1)S(1)} %bitcast.180, bf16[512,384]{1,0:T(8,128)(2,1)S(1)} %get-tuple-element.22), kind=kOutput, calls=%fused_computation.5 | convolution fusion | flops 806092800 | bytes 4063232 | tf_op jit(solution)/shard_map/rd,rf->df/dot_general | solution.py:600
  57.3 2.2 %fusion.2 = bf16[1,384,2048]{2,1,0:T(8,128)(2,1)} fusion(bf16[512,2048]{1,0:T(8,128)(2,1)S(1)} %bitcast.176, f32[512,384]{1,0:T(8,128)S(1)} %fusion.8, f32[512,384]{1,0:T(8,128)S(1)} %fusion.5), kind=kOutput, calls=%fused_computation.6 | convolution fusion | flops 807272448 | bytes 5242880 | tf_op jit(solution)/shard_map/rf,rd->fd/dot_general | solution.py:591
  59.5 1.0 copy.84
  60.5 1.3 fusion.3
  61.9 2.6 %add_convert_fusion = bf16[512,2048]{1,0:T(8,128)(2,1)} fusion(f32[512,2048]{1,0:T(8,128)S(1)} %fusion.3, bf16[512,384]{1,0:T(8,128)(2,1)S(1)} %get-tuple-element.22, bf16[1,2048,384]{2,1,0:T(8,128)(2,1)S(1)} %copy-done.10), kind=kOutput, calls=%fused_computation | convolution fusion | flops 807403520 | bytes 8257536 | tf_op jit(solution)/shard_map/rf,df->rd/dot_general | solution.py:604
  64.8 0.1 reshape.191
  65.0 0.4 convolution_bitcast_fusion.6
  65.5 0.5 convolution_select_fusion.1
  66.0 0.3 multiply_reduce_fusion.1
  66.4 0.6 copy-done.25
  67.2 34.8 %give_back.1 = (bf16[8,64,512]{2,1,0:T(8,128)(2,1)S(1)}, bf16[8,128,256]{2,1,0:T(8,128)(2,1)S(1)}) custom-call(bf16[8,64,2048]{2,1,0:T(8,128)(2,1)S(1)} %bitcast.170, bf16[128,256]{1,0:T(8,128)(2,1)S(1)} %bitcast.174), custom_call_target="tpu_custom_call" | custom-call | tf_op jit(solution)/shard_map/give_back/pallas_call | solution.py:362
  102.0 0.9 fusion.15.x_ref
  103.0 8.4 %all_features.1 = bf16[4,128,512]{2,1,0:T(8,128)(2,1)} custom-call(bf16[128,512]{1,0:T(8,128)(2,1)} %fusion.15.x_ref), custom_call_target="tpu_custom_call" | custom-call | tf_op jit(solution)/shard_map/all_features/pallas_call | solution.py:415
  111.4 2.2 %convert_bitcast_fusion = f32[128,4,512]{2,0,1:T(8,128)} fusion(bf16[4,128,512]{2,1,0:T(8,128)(2,1)} %all_features.1), kind=kLoop, calls=%fused_computation.53 | loop fusion | flops 262144 | bytes 1572864 | tf_op jit(solution)/shard_map/reshape | solution.py:616
  113.5 1.5 copy.97
  115.1 1.4 fusion.25
  116.5 2.4 %fusion.29 = bf16[128,2048]{0,1:T(8,128)(2,1)} fusion(bf16[128,2048]{0,1:T(8,128)(2,1)} %copy-done.2, bf16[128,2048]{0,1:T(8,128)(2,1)} %copy.84, f32[128,4,512]{0,2,1:T(8,128)S(1)} %copy.97, f32[128]{0:T(128)S(1)} %broadcast_multiply_fusion.3, f32[2048]{0:T(1024)} %param.15, f32[128]{0:T(128)S(1)} %copy-done.42), kind=kLoop, calls=%fused_computation.50 | loop fusion | flops 2359296 | bytes 2630656 | tf_op jit(solution)/shard_map/convert_element_type | solution.py:621
  119.0 1.3 copy.98
  120.2 1.8 %convolution_convert_fusion.4 = bf16[128,256]{1,0:T(8,128)(2,1)S(1)} fusion(bf16[128,2048]{0,1:T(8,128)(2,1)} %fusion.29, bf16[2048,256]{1,0:T(8,128)(2,1)} %param.22), kind=kOutput, calls=%fused_computation.43 | convolution fusion | flops 134250496 | bytes 1638400 | tf_op jit(solution)/shard_map/dot_general | solution.py:622
  122.1 0.2 multiply_reduce_fusion
  122.3 0.8 subtract_multiply_fusion
  123.2 0.3 fusion.59
  123.5 0.8 fusion.43
  124.4 23.5 %last_exchange.1 = (bf16[8,128,256]{2,1,0:T(8,128)(2,1)S(1)}, f32[136,128]{1,0:T(8,128)S(1)}) custom-call(bf16[8,128,256]{2,1,0:T(8,128)(2,1)S(1)} %bitcast.173, f32[136,128]{1,0:T(8,128)S(1)} %pad_maximum_fusion.state_ref), custom_call_target="tpu_custom_call" | custom-call | tf_op jit(solution)/shard_map/last_exchange/pallas_call | solution.py:454
  147.9 1.0 convolution_bitcast_fusion
  148.9 1.3 fusion.20
  150.2 0.2 convolution_select_fusion
  150.5 0.4 fusion.19
  150.9 1.0 slice_add_fusion
  152.0 1.0 fusion.16
  153.0 0.3 multiply_subtract_fusion
  153.5 0.7 convert_element_type.104
  154.3 0.7 convert_element_type.106
  155.0 0.4 fusion.81
  155.4 0.5 fusion.24
  156.0 0.6 copy.138
  156.7 0.1 reshape.187
  156.9 1.1 reduce_window_sum.34
  158.1 0.2 multiply_reduce_fusion.2
  158.3 0.6 broadcast_add_fusion
  (127 shorter events, 2.3 us)
Async XLA Ops:
  0.6 47.5 %copy-start = (bf16[1,2048,384]{2,1,0:T(8,128)(2,1)S(1)}, bf16[1,2048,384]{2,1,0:T(8,128)(2,1)}, u32[]{:S(2)}) copy-start(bf16[1,2048,384]{2,1,0:T(8,128)(2,1)} %param.19) | copy-start | bytes 4718596
  0.6 5.5 %copy-start.43 = (s32[128,2]{0,1:T(2,128)S(1)}, s32[128,2]{0,1:T(2,128)}, u32[]{:S(2)}) copy-start(s32[128,2]{0,1:T(2,128)} %param.16) | copy-start | bytes 3076
  0.7 5.4 %copy-start.40 = (f32[128,2]{0,1:T(2,128)S(1)}, f32[128,2]{0,1:T(2,128)}, u32[]{:S(2)}) copy-start(f32[128,2]{0,1:T(2,128)} %param.17) | copy-start | bytes 3076
  0.7 6.9 %copy-start.19 = (f32[128,128]{1,0:T(8,128)S(1)}, f32[128,128]{1,0:T(8,128)}, u32[]{:S(2)}) copy-start(f32[128,128]{1,0:T(8,128)} %param.26) | copy-start | bytes 196612
  0.7 7.3 %copy-start.20 = (bf16[128,256]{1,0:T(8,128)(2,1)S(1)}, bf16[128,256]{1,0:T(8,128)(2,1)}, u32[]{:S(2)}) copy-start(bf16[128,256]{1,0:T(8,128)(2,1)} %param.25) | copy-start | bytes 196612
  0.7 7.3 %copy-start.27 = (bf16[128,128]{1,0:T(8,128)(2,1)S(1)}, bf16[128,128]{1,0:T(8,128)(2,1)}, u32[]{:S(2)}) copy-start(bf16[128,128]{1,0:T(8,128)(2,1)} %param.24) | copy-start | bytes 98308
  4.0 0.8 copy-start.2
  4.8 2.8 %copy-start.41 = (f32[128]{0:T(128)}, f32[128]{0:T(128)S(1)}, u32[]{:S(2)}) copy-start(f32[128]{0:T(128)S(1)} %add_rsqrt_fusion.1) | copy-start | bytes 1540
  7.8 2.5 %copy-start.31 = (f32[2,2,64]{2,1,0:T(2,128)}, f32[2,2,64]{2,1,0:T(2,128)S(1)}, u32[]{:S(2)}) copy-start(f32[2,2,64]{2,1,0:T(2,128)S(1)} %fusion.78) | copy-start | bytes 3076
  7.9 3.1 %copy-start.21 = (f32[8,128]{1,0:T(8,128)}, f32[8,128]{1,0:T(8,128)S(1)}, u32[]{:S(2)}) copy-start(f32[8,128]{1,0:T(8,128)S(1)} %broadcast_in_dim.96) | copy-start | bytes 12292
  8.0 58.0 %copy-start.5 = (bf16[2,64,2,128]{3,2,1,0:T(2,128)(2,1)}, bf16[2,64,2,128]{3,2,1,0:T(2,128)(2,1)S(1)}, u32[]{:S(2)}) copy-start(bf16[2,64,2,128]{3,2,1,0:T(2,128)(2,1)S(1)} %reshape.173) | copy-start | bytes 196612
  8.3 2.0 %copy-start.23 = (f32[2,2,64]{2,1,0:T(2,128)}, f32[2,2,64]{2,1,0:T(2,128)S(1)}, u32[]{:S(2)}) copy-start(f32[2,2,64]{2,1,0:T(2,128)S(1)} %get-tuple-element.28) | copy-start | bytes 3076
  8.6 55.9 %copy-start.7 = (f32[2,2,64,128]{3,2,1,0:T(8,128)}, f32[2,2,64,128]{3,2,1,0:T(8,128)S(1)}, u32[]{:S(2)}) copy-start(f32[2,2,64,128]{3,2,1,0:T(8,128)S(1)} %fusion.63) | copy-start | bytes 393220
  9.2 55.8 %copy-start.30 = (f32[2,2,64]{2,1,0:T(2,128)}, f32[2,2,64]{2,1,0:T(2,128)S(1)}, u32[]{:S(2)}) copy-start(f32[2,2,64]{2,1,0:T(2,128)S(1)} %get-tuple-element.29) | copy-start | bytes 3076
  9.8 0.7 copy-start.33
  10.4 0.5 copy-start.38
  48.2 1.4 copy-start.9
  49.6 1.4 copy-start.44
  57.3 2.2 %copy-start.16 = (bf16[128,2048]{1,0:T(8,128)(2,1)S(1)}, bf16[128,2048]{1,0:T(8,128)(2,1)}, u32[]{:S(2)}) copy-start(bf16[128,2048]{1,0:T(8,128)(2,1)} %param.18) | copy-start | bytes 1572868
  60.5 1.4 copy-start.10
  61.9 2.6 %copy-start.34 = (f32[2,64]{1,0:T(2,128)S(1)}, f32[2,64]{1,0:T(2,128)}, u32[]{:S(2)}) copy-start(f32[2,64]{1,0:T(2,128)} %copy-done.33) | copy-start | bytes 1540
  61.9 2.9 %copy-start.28 = (bf16[128,128]{1,0:T(8,128)(2,1)S(1)}, bf16[128,128]{1,0:T(8,128)(2,1)}, u32[]{:S(2)}) copy-start(bf16[128,128]{1,0:T(8,128)(2,1)} %param.23) | copy-start | bytes 98308
  64.5 2.4 %copy-start.36 = (f32[256]{0:T(256)S(1)}, f32[256]{0:T(256)}, u32[]{:S(2)}) copy-start(f32[256]{0:T(256)} %param.27) | copy-start | bytes 3076
  64.6 37.4 %copy-start.18 = (f32[1,2,64,128]{3,2,1,0:T(8,128)}, f32[1,2,64,128]{3,2,1,0:T(8,128)S(1)}, u32[]{:S(2)}) copy-start(f32[1,2,64,128]{3,2,1,0:T(8,128)S(1)} %slice_add_fusion.1) | copy-start | bytes 196612
  64.8 0.7 copy-start.13
  65.0 2.1 %copy-start.1 = (bf16[512,2048]{1,0:T(8,128)(2,1)S(1)}, bf16[512,2048]{1,0:T(8,128)(2,1)}, u32[]{:S(2)}) copy-start(bf16[512,2048]{1,0:T(8,128)(2,1)} %add_convert_fusion) | copy-start | bytes 6291460
  66.0 45.4 %copy-start.11 = (f32[2,2,64,64]{3,2,1,0:T(8,128)}, f32[2,2,64,64]{3,2,1,0:T(8,128)S(1)}, u32[]{:S(2)}) copy-start(f32[2,2,64,64]{3,2,1,0:T(8,128)S(1)} %convolution_select_fusion.1) | copy-start | bytes 196612
  66.3 0.8 copy-start.3
  66.3 0.6 copy-start.25
  103.0 12.1 %copy-start.42 = (f32[128]{0:T(128)S(1)}, f32[128]{0:T(128)}, u32[]{:S(2)}) copy-start(f32[128]{0:T(128)} %copy-done.41) | copy-start | bytes 1540
  118.9 3.2 %copy-start.4 = (f32[2,64,2,128]{3,1,2,0:T(8,128)S(1)}, f32[2,64,2,128]{3,1,2,0:T(8,128)}, u32[]{:S(2)}) copy-start(f32[2,64,2,128]{3,1,2,0:T(8,128)} %copy-done.3) | copy-start | bytes 393220
  118.9 3.2 %copy-start.26 = (f32[2,64,2]{1,2,0:T(2,128)S(1)}, f32[2,64,2]{1,2,0:T(2,128)}, u32[]{:S(2)}) copy-start(f32[2,64,2]{1,2,0:T(2,128)} %copy-done.25) | copy-start | bytes 3076
  118.9 3.2 %copy-start.37 = (f32[256]{0:T(256)S(1)}, f32[256]{0:T(256)}, u32[]{:S(2)}) copy-start(f32[256]{0:T(256)} %param.27) | copy-start | bytes 3076
  118.9 5.4 %copy-start.22 = (f32[8,128]{1,0:T(8,128)S(1)}, f32[8,128]{1,0:T(8,128)}, u32[]{:S(2)}) copy-start(f32[8,128]{1,0:T(8,128)} %copy-done.21) | copy-start | bytes 12292
  122.0 26.9 %copy-start.14 = (f32[128,128]{0,1:T(8,128)S(1)}, f32[128,128]{0,1:T(8,128)}, u32[]{:S(2)}) copy-start(f32[128,128]{0,1:T(8,128)} %copy-done.13) | copy-start | bytes 196612
  122.1 28.1 %copy-start.6 = (bf16[2,64,2,128]{3,2,1,0:T(2,128)(2,1)S(1)}, bf16[2,64,2,128]{3,2,1,0:T(2,128)(2,1)}, u32[]{:S(2)}) copy-start(bf16[2,64,2,128]{3,2,1,0:T(2,128)(2,1)} %copy-done.5) | copy-start | bytes 196612
  123.5 27.0 %copy-start.17 = (f32[2,2,64,128]{3,2,1,0:T(8,128)}, f32[2,2,64,128]{3,2,1,0:T(8,128)S(1)}, u32[]{:S(2)}) copy-start(f32[2,2,64,128]{3,2,1,0:T(8,128)S(1)} %fusion.59) | copy-start | bytes 393220
  148.9 6.1 %copy-start.12 = (f32[2,2,64,64]{3,2,1,0:T(8,128)S(1)}, f32[2,2,64,64]{3,2,1,0:T(8,128)}, u32[]{:S(2)}) copy-start(f32[2,2,64,64]{3,2,1,0:T(8,128)} %copy-done.11) | copy-start | bytes 196612
  148.9 6.5 %copy-start.24 = (f32[2,2,64]{2,1,0:T(2,128)S(1)}, f32[2,2,64]{2,1,0:T(2,128)}, u32[]{:S(2)}) copy-start(f32[2,2,64]{2,1,0:T(2,128)} %copy-done.23) | copy-start | bytes 3076
  148.9 6.5 %copy-start.29 = (f32[2,2,64]{2,1,0:T(2,128)S(1)}, f32[2,2,64]{2,1,0:T(2,128)}, u32[]{:S(2)}) copy-start(f32[2,2,64]{2,1,0:T(2,128)} %get-tuple-element.31) | copy-start | bytes 3076
  150.9 7.1 %copy-start.32 = (f32[2,2,64]{2,1,0:T(2,128)S(1)}, f32[2,2,64]{2,1,0:T(2,128)}, u32[]{:S(2)}) copy-start(f32[2,2,64]{2,1,0:T(2,128)} %copy-done.31) | copy-start | bytes 3076
  150.9 7.1 %copy-start.8 = (f32[2,2,64,128]{3,2,1,0:T(8,128)S(1)}, f32[2,2,64,128]{3,2,1,0:T(8,128)}, u32[]{:S(2)}) copy-start(f32[2,2,64,128]{3,2,1,0:T(8,128)} %copy-done.7) | copy-start | bytes 393220
  150.9 7.1 %copy-start.15 = (f32[128,128]{0,1:T(8,128)S(1)}, f32[128,128]{0,1:T(8,128)}, u32[]{:S(2)}) copy-start(f32[128,128]{0,1:T(8,128)} %copy-done.13) | copy-start | bytes 196612
  150.9 7.1 %copy-start.35 = (f32[2,64]{1,0:T(2,128)S(1)}, f32[2,64]{1,0:T(2,128)}, u32[]{:S(2)}) copy-start(f32[2,64]{1,0:T(2,128)} %copy-done.33) | copy-start | bytes 1540
  150.9 7.1 %copy-start.39 = (f32[2,64]{1,0:T(2,128)S(1)}, f32[2,64]{1,0:T(2,128)}, u32[]{:S(2)}) copy-start(f32[2,64]{1,0:T(2,128)} %copy-done.38) | copy-start | bytes 1540

commit v2 on v1

--- a/solution.py
+++ b/solution.py
@@ -124,8 +124,11 @@
 
 def dispatch_kernel(
     n,
-    a_ref,
-    b_ref,
+    hidden_ref,
+    cot_ref,
+    gain_ref,
+    pick_ref,
+    weight_ref,
     state_ref,
     a_out,
     b_out,
@@ -134,6 +137,9 @@
     sent,
     carry_send,
     carry_recv,
+    a_ref,
+    b_ref,
+    normed,
     local_sem,
     send_sem,
     recv_sem,
@@ -186,9 +192,24 @@
         forward(j, k, 0).start()
         forward(j, k, 1).start()
 
+    def fill(j, block):
+        chosen = pick_ref[block]
+        if j == 0:
+            rows = jnp.dot(chosen, normed[...], preferred_element_type=jnp.float32)
+        else:
+            rows = jnp.dot(chosen, cot_ref[:, lanes(tp)], preferred_element_type=jnp.float32)
+            rows = rows * weight_ref[block]
+        ins[j][block] = rows.astype(jnp.bfloat16)
+
     def begin(j):
+        fill(j, lax.rem(me + 1, n))
+
+        def one(k):
+            fill(j, lax.rem(me + k + 1, n))
+            exchange(j, k).start()
+
+        each(1, n, one)
         own(j).start()
-        each(1, n, lambda k: exchange(j, k).start())
         own(j).wait()
         forward(j, 0, 0).start()
         forward(j, 0, 1).start()
@@ -200,6 +221,10 @@
 
     half = n // 2
     carry.send(0)
+    every = hidden_ref[...].astype(jnp.float32)
+    row_scale = lax.rsqrt(jnp.mean(every * every, axis=-1, keepdims=True) + eps_value)
+    mine = hidden_ref[:, lanes(tp)].astype(jnp.float32) * row_scale * gain_ref[:, lanes(tp)]
+    normed[...] = mine.astype(jnp.bfloat16)
     begin(0)
     carry.receive(0, steps == 1)
     if steps > 1:
@@ -231,17 +256,22 @@
     return [pl.BlockSpec(memory_space=pltpu.VMEM)] * count
 
 
-def dispatch(n, part_in, part_grad, packed):
-    count, cap, width = part_in.shape
-    full = jax.ShapeDtypeStruct((count, cap, 4 * width), part_in.dtype)
+def dispatch(n, hidden, cot, gain, pick, weight, packed):
+    count, cap = pick.shape[:2]
+    width = hidden.shape[1] // 4
+    part = pltpu.VMEM((count, cap, width), jnp.bfloat16)
+    full = jax.ShapeDtypeStruct((count, cap, 4 * width), jnp.bfloat16)
     dma = pltpu.SemaphoreType.DMA
     return pl.pallas_call(
         functools.partial(dispatch_kernel, n),
         out_shape=[full, full, jax.ShapeDtypeStruct(packed.shape, jnp.float32)],
-        in_specs=vmem(3),
+        in_specs=vmem(6),
         out_specs=vmem(3),
         scratch_shapes=carry_scratch(n, packed.shape)
         + [
+            part,
+            part,
+            pltpu.VMEM((hidden.shape[0], width), jnp.bfloat16),
             dma((2,)),
             dma((2, n)),
             dma((2, n)),
@@ -254,15 +284,25 @@
             collective_id=0, has_side_effects=True, vmem_limit_bytes=40 << 20
         ),
         name="dispatch",
-    )(part_in, part_grad, packed)
+    )(hidden, cot, gain, pick, weight, packed)
 
 
 def return_kernel(
     n,
     part_ref,
     mix_ref,
+    pick_ref,
+    hidden_ref,
+    cot_ref,
+    gain_ref,
+    w_ref,
+    mixed_grad_out,
+    mix_grad_out,
+    mix_out,
     back_out,
-    mix_out,
+    summed,
+    features,
+    mixed_grad,
     near,
     far_sum,
     far,
@@ -276,6 +316,8 @@
     recv_sem,
     mix_send,
     mix_recv,
+    feature_send,
+    feature_recv,
 ):
     me, tp = lax.axis_index("sp"), lax.axis_index("tp")
     pair, twin = tp_pair(tp)
@@ -305,15 +347,27 @@
         block = lax.rem(me + k, n)
         return remote(total.at[block], back_out.at[me], send_sem.at[k], recv_sem.at[k], block, tp)
 
-    def mixed(k):
-        to = lax.rem(me + k, n)
-        return remote(mix_ref, mix_out.at[me], mix_send.at[k], mix_recv.at[k], to, tp)
+    mix_steps = (n - 1).bit_length()
+
+    def mixed(step, j, from_me):
+        d = n >> (step + 1)
+        other = me + d * (1 - 2 * lax.rem(lax.div(me, d), 2))
+        block = lax.rem(me if from_me else other, 2 * d) + 2 * d * j
+        piece = mix_out.at[block]
+        return remote(piece, piece, mix_send.at[step, j], mix_recv.at[block], other, tp)
+
+    def mix_start(step):
+        each(0, 1 << step, lambda j: mixed(step, j, True).start())
+
+    def mix_finish(step):
+        each(0, 1 << step, lambda j: mixed(step, j, False).wait_recv())
 
     each(1, n + 1, lambda k: to_pair(1, lax.rem(k, n)).start())
     each(1, n + 1, lambda k: to_pair(0, lax.rem(k, n)).start())
-    each(1, n, lambda k: mixed(k).start())
     own_mix = pltpu.make_async_copy(mix_ref, mix_out.at[me], local_sem.at[0])
     own_mix.start()
+    own_mix.wait()
+    mix_start(0)
 
     def reduce_pair(i):
         k = lax.rem(i, n)
@@ -325,6 +379,9 @@
 
     each(1, n + 1, reduce_pair)
     to_twin(0).start()
+    mix_finish(0)
+    if mix_steps > 1:
+        mix_start(1)
 
     def reduce_all(i):
         k = lax.rem(i, n)
@@ -338,8 +395,32 @@
 
     each(1, n + 1, reduce_all)
     back_out[me] = total[me]
-    own_mix.wait()
-
+    if mix_steps > 1:
+        mix_finish(1)
+    for step in range(2, mix_steps):
+        mix_start(step)
+        if step + 1 < mix_steps:
+            mix_finish(step)
+
+    summed[...] = jnp.dot(pick_ref[me], back_out[me], preferred_element_type=jnp.float32)
+
+    def gather(k):
+        block = lax.rem(me - k + n, n)
+        to_owner(k).wait_recv()
+        summed[...] += jnp.dot(
+            pick_ref[block], back_out[block], preferred_element_type=jnp.float32
+        )
+
+    each(1, n, gather)
+    features[tp] = summed[...].astype(jnp.bfloat16)
+    spread = [
+        remote(
+            features.at[q], features.at[q], feature_send.at[i], feature_recv.at[i], me, other
+        )
+        for i, (q, other) in enumerate([(tp, twin), (tp, pair), (twin, pair)])
+    ]
+    spread[0].start()
+    spread[1].start()
     def finish(k):
         for kind in (0, 1):
             to_pair(kind, k).wait_send()
@@ -348,26 +429,62 @@
     each(0, n, finish)
 
     def finish_far(k):
-        to_owner(k).wait()
-        mixed(k).wait()
+        to_owner(k).wait_send()
 
     each(1, n, finish_far)
-
-
-def give_back(n, partial_rows, mixed_out):
+    if mix_steps > 2:
+        mix_finish(mix_steps - 1)
+    for step in range(mix_steps):
+        each(0, 1 << step, lambda j, step=step: mixed(step, j, True).wait_send())
+    spread[0].wait_recv()
+    spread[2].start()
+    spread[1].wait()
+    spread[2].wait()
+    spread[0].wait_send()
+    rows = 32
+    parts = mixed_grad_out.shape[0]
+
+    def grads(i):
+        here = pl.ds(pl.multiple_of(i * rows, rows), rows)
+        state = hidden_ref[here, :].astype(jnp.float32)
+        row_scale = lax.rsqrt(jnp.mean(state * state, axis=-1, keepdims=True) + eps_value)
+        unit = state * row_scale
+        back = jnp.concatenate([features[q, here, :] for q in range(4)], axis=1)
+        grad = back.astype(jnp.float32) * gain_ref[...]
+        grad = row_scale * (grad - unit * jnp.mean(grad * unit, axis=-1, keepdims=True))
+        mixed_rows = (cot_ref[here, :].astype(jnp.float32) + grad).astype(jnp.bfloat16)
+        mixed_grad[here, :] = mixed_rows
+        piece = mixed_rows.shape[1] // parts
+        for q in range(parts):
+            mixed_grad_out[q, here, :] = mixed_rows[:, q * piece : (q + 1) * piece]
+
+    each(0, hidden_ref.shape[0] // rows, grads)
+    mix_grad_out[...] = jnp.dot(
+        mixed_grad[...], w_ref[...], preferred_element_type=jnp.float32
+    ).astype(jnp.bfloat16)
+
+
+def give_back(n, partial_rows, mixed_out, pick, hidden, cot, gain, w_out):
     count, cap, model_width = partial_rows.shape
+    tokens = hidden.shape[0]
+    parts = n if (model_width // n) % 128 == 0 else 1
     width = model_width // 4
     dma = pltpu.SemaphoreType.DMA
     block = (count, cap, width)
     return pl.pallas_call(
         functools.partial(return_kernel, n),
         out_shape=[
-            jax.ShapeDtypeStruct(block, jnp.bfloat16),
+            jax.ShapeDtypeStruct((parts, tokens, model_width // parts), jnp.bfloat16),
+            jax.ShapeDtypeStruct(mixed_out.shape, jnp.bfloat16),
             jax.ShapeDtypeStruct((n,) + mixed_out.shape, jnp.bfloat16),
         ],
-        in_specs=vmem(2),
-        out_specs=vmem(2),
+        in_specs=vmem(7),
+        out_specs=vmem(3),
         scratch_shapes=[
+            pltpu.VMEM(block, jnp.bfloat16),
+            pltpu.VMEM((tokens, width), jnp.float32),
+            pltpu.VMEM((4, tokens, width), jnp.bfloat16),
+            pltpu.VMEM((tokens, model_width), jnp.bfloat16),
             pltpu.VMEM((2,) + block, jnp.bfloat16),
             pltpu.VMEM(block, jnp.bfloat16),
             pltpu.VMEM(block, jnp.bfloat16),
@@ -379,74 +496,94 @@
             dma((n,)),
             dma((n,)),
             dma((n,)),
+            dma(((n - 1).bit_length(), max(1, n // 2))),
             dma((n,)),
-            dma((n,)),
+            dma((3,)),
+            dma((3,)),
         ],
         compiler_params=pltpu.CompilerParams(
             collective_id=1, has_side_effects=True, vmem_limit_bytes=40 << 20
         ),
         name="give_back",
-    )(partial_rows, mixed_out)
-
-
-def features_kernel(x_ref, out_ref, local_sem, send_sem, recv_sem):
+    )(partial_rows, mixed_out, pick, hidden, cot, gain, w_out)
+
+
+def last_kernel(
+    n,
+    rows_ref,
+    state_ref,
+    rows_out,
+    scan_out,
+    held,
+    sent,
+    carry_send,
+    carry_recv,
+    local_sem,
+    send_sem,
+    recv_sem,
+    pair_send,
+    pair_recv,
+    twin_send,
+    twin_recv,
+):
     me, tp = lax.axis_index("sp"), lax.axis_index("tp")
     pair, twin = tp_pair(tp)
-    greet(1, me, tp, [(me, pair), (me, twin)])
-    own = pltpu.make_async_copy(x_ref, out_ref.at[tp], local_sem.at[0])
-    own.start()
-    copies = [
-        remote(x_ref, out_ref.at[tp], send_sem.at[0], recv_sem.at[0], me, twin),
-        remote(x_ref, out_ref.at[tp], send_sem.at[1], recv_sem.at[1], me, pair),
-        remote(out_ref.at[twin], out_ref.at[twin], send_sem.at[2], recv_sem.at[2], me, pair),
-    ]
-    copies[0].start()
-    copies[1].start()
-    copies[0].wait_recv()
-    copies[2].start()
-    copies[1].wait()
-    copies[2].wait()
-    copies[0].wait_send()
-    own.wait()
-
-
-def all_features(x):
-    dma = pltpu.SemaphoreType.DMA
-    return pl.pallas_call(
-        features_kernel,
-        out_shape=jax.ShapeDtypeStruct((4,) + x.shape, x.dtype),
-        in_specs=vmem(1),
-        out_specs=pl.BlockSpec(memory_space=pltpu.VMEM),
-        scratch_shapes=[dma((1,)), dma((3,)), dma((3,))],
-        compiler_params=pltpu.CompilerParams(collective_id=2, has_side_effects=True),
-        name="all_features",
-    )(x)
-
-
-def last_kernel(
-    n, rows_ref, state_ref, rows_out, scan_out, held, sent, carry_send, carry_recv, local_sem, send_sem, recv_sem
-):
-    me, tp = lax.axis_index("sp"), lax.axis_index("tp")
-    greet(n, me, tp, [])
+    greet(n, me, tp, [(me, pair), (me, twin)])
+    share = rows_ref.shape[1] // 4
+
+    def rows_of(t):
+        return pl.ds(pl.multiple_of(t * share, share), share)
+
     steps = steps_of(n)
     carry = Carry(n, me, tp, True, state_ref, held, sent, scan_out, carry_send, carry_recv)
 
     def exchange(k):
         to = lax.rem(me + k, n)
-        return remote(rows_ref.at[to], rows_out.at[me], send_sem.at[k], recv_sem.at[k], to, tp)
+        return remote(
+            rows_ref.at[to, rows_of(tp)],
+            rows_out.at[me, rows_of(tp)],
+            send_sem.at[k],
+            recv_sem.at[k],
+            to,
+            tp,
+        )
+
+    def forward(k, kind):
+        block = lax.rem(me - k + n, n)
+        piece = rows_out.at[block, rows_of(twin if kind == 2 else tp)]
+        if kind == 0:
+            return remote(piece, piece, twin_send.at[k], twin_recv.at[k], me, twin)
+        return remote(piece, piece, pair_send.at[kind - 1, k], pair_recv.at[kind - 1, k], me, pair)
+
+    def spread(k):
+        exchange(k).wait_recv()
+        forward(k, 0).start()
+        forward(k, 1).start()
+
+    def twin_done(k):
+        forward(k, 0).wait_recv()
+        forward(k, 2).start()
+
+    def finish(k):
+        exchange(k).wait_send()
+        forward(k, 0).wait_send()
+        forward(k, 1).wait()
+        forward(k, 2).wait()
 
     own = pltpu.make_async_copy(rows_ref.at[me], rows_out.at[me], local_sem.at[0])
     carry.send(0)
     own.start()
-    cuts = [1 + (n - 1) * i // steps for i in range(steps + 1)]
+    each(1, n, lambda k: exchange(k).start())
     for step in range(steps):
-        each(cuts[step], cuts[step + 1], lambda k: exchange(k).start())
         carry.receive(step, step == steps - 1)
         if step + 1 < steps:
             carry.send(step + 1)
+        if step == 0:
+            each(1, n, spread)
+    each(1, n, twin_done)
     carry.finish(steps)
     own.wait()
-    each(1, n, lambda k: exchange(k).wait())
+    each(1, n, finish)
 
 
 def last_exchange(n, rows, packed):
@@ -459,7 +596,15 @@
         ],
         in_specs=vmem(2),
         out_specs=vmem(2),
-        scratch_shapes=carry_scratch(n, packed.shape) + [dma((1,)), dma((n,)), dma((n,))],
+        scratch_shapes=carry_scratch(n, packed.shape) + [
+            dma((1,)),
+            dma((n,)),
+            dma((n,)),
+            dma((2, n)),
+            dma((2, n)),
+            dma((n,)),
+            dma((n,)),
+        ],
         compiler_params=pltpu.CompilerParams(
             collective_id=3, has_side_effects=True, vmem_limit_bytes=40 << 20
         ),
@@ -533,14 +678,6 @@
     ones_decay = jnp.ones_like(total_log)
     local_end, local_start = block_scan(block_decay, block_kv, zero_state, False)
     sp_count = lax.axis_size("sp")
-    state_f = hidden_state.astype(jnp.float32)
-    row_scale = lax.rsqrt(jnp.mean(state_f * state_f, axis=-1, keepdims=True) + eps_value)
-    part_width = model_width // lax.axis_size("tp")
-    feature_start = lax.axis_index("tp") * part_width
-    hidden_part = lax.dynamic_slice_in_dim(hidden_state, feature_start, part_width, 1)
-    gain_part = lax.dynamic_slice_in_dim(norm_gain, feature_start, part_width, 0)
-    cot_part = lax.dynamic_slice_in_dim(cotangent, feature_start, part_width, 1)
-    normed_part = (hidden_part.astype(jnp.float32) * row_scale * gain_part).astype(jnp.bfloat16)
     route_weight = jax.nn.softmax(route_logits, axis=-1)
     expert_count = sp_count
     capacity = 4 * tok_count // expert_count
@@ -552,14 +689,13 @@
     place = jnp.where(names, rank, -1.0).T
     filled = place[:, None, :] == jnp.arange(capacity, dtype=jnp.float32)[None, :, None]
     slot_weight = jnp.sum(jnp.where(filled, weight_of.T[:, None, :], 0.0), axis=2)
-    pick = filled.astype(jnp.bfloat16).reshape(expert_count * capacity, tok_count)
-    send_in = jnp.dot(pick, normed_part, preferred_element_type=jnp.float32).astype(jnp.bfloat16)
-    send_grad = jnp.dot(pick, cot_part, preferred_element_type=jnp.float32)
-    send_grad = (send_grad * slot_weight.reshape(-1, 1)).astype(jnp.bfloat16)
     got_in, got_grad, scanned = dispatch(
         sp_count,
-        send_in.reshape(expert_count, capacity, part_width),
-        send_grad.reshape(expert_count, capacity, part_width),
+        hidden_state,
+        cotangent,
+        norm_gain.reshape(1, -1),
+        filled.astype(jnp.bfloat16),
+        slot_weight[:, :, None],
         pack_state(local_end, total_decay),
     )
     state_in = unpack_state(scanned, head_count)
@@ -576,8 +712,6 @@
     normed = head_out * inv_rms
     gain_heads = head_gain.reshape(head_count, VAL_DIM)
     mixed_out = (normed * gain_heads).reshape(tok_count, head_count * VAL_DIM).astype(jnp.bfloat16)
-    unit_rows = state_f * row_scale
-    cot_f = cotangent.astype(jnp.float32)
     rows_in = got_in.reshape(-1, model_width)
     rows_grad = got_grad.reshape(-1, model_width)
     gate_w = w_gate[0]
@@ -605,29 +739,25 @@
         "rf,df->rd", grad_up_pre, up_w, preferred_element_type=jnp.float32
     )
     partial_rows = partial_rows.reshape(expert_count, capacity, model_width)
-    returned, mixed_all = give_back(sp_count, partial_rows.astype(jnp.bfloat16), mixed_out)
-    summed = lax.dot_general(
-        pick,
-        returned.reshape(-1, part_width),
-        (((0,), (0,)), ((), ())),
-        preferred_element_type=jnp.float32,
-    )
-    grad_normed = all_features(summed.astype(jnp.bfloat16)).astype(jnp.float32)
-    grad_normed = grad_normed.transpose(1, 0, 2).reshape(tok_count, model_width)
-    grad_unit = grad_normed * norm_gain
-    grad_state = row_scale * (
-        grad_unit - unit_rows * jnp.mean(grad_unit * unit_rows, axis=-1, keepdims=True)
-    )
-    grad_mixed = (cot_f + grad_state).astype(jnp.bfloat16)
-    grad_mix = jnp.dot(grad_mixed, w_out, preferred_element_type=jnp.float32).astype(jnp.bfloat16)
-    grad_mix = lax.optimization_barrier(grad_mix).astype(jnp.float32).reshape(shape_value)
+    mixed_parts, grad_mix, mixed_all = give_back(
+        sp_count,
+        partial_rows.astype(jnp.bfloat16),
+        mixed_out,
+        (place[:, :, None] == jnp.arange(capacity, dtype=jnp.float32)).astype(jnp.bfloat16),
+        hidden_state,
+        cotangent,
+        norm_gain.reshape(1, -1),
+        w_out,
+    )
+    if mixed_parts.shape[0] != sp_count:
+        mixed_parts = mixed_parts.reshape(tok_count, sp_count, -1).transpose(1, 0, 2)
+    grad_mix = grad_mix.astype(jnp.float32).reshape(shape_value)
     grad_scaled = grad_mix * gain_heads
     grad_out = inv_rms * (
         grad_scaled - normed * jnp.mean(grad_scaled * normed, axis=-1, keepdims=True)
     )
     block_adj = jnp.einsum("bthk,bthv->bhkv", query_start, grad_out, precision=exact_numeric_mode)
     local_adj, later_adj = block_scan(block_decay, block_adj, zero_state, True)
-    mixed_parts = grad_mixed.reshape(tok_count, sp_count, -1).transpose(1, 0, 2)
     got_mixed, behind = last_exchange(sp_count, mixed_parts, pack_state(local_adj, total_decay))
     grad_out_w = jnp.einsum("ntd,nth->dh", got_mixed, mixed_all, preferred_element_type=jnp.float32)
     adj_end = unpack_state(behind, head_count)

time: 160 us -> 144 us (0.900)
  Pallas kernels: 104 us -> 94.8 us
  matrix products: 27.1 us -> 22.2 us
    pallas_call x1 -> x0, Pallas kernels: 8.4 us -> none  [all_features(): pl.pallas_call(features_kernel, out_shape=jax.ShapeDtypeStruct((4,) + x.s...]
    pallas_call x1, Pallas kernels: 23.5 us -> 17.1 us  [last_exchange(): pl.pallas_call(functools.partial(last_kernel, n), out_shape=[jax.ShapeDty...]
    dot_general x4 -> x0, matrix products: 5.16 us -> none  [the longest x1 1.76 us: body(): jnp.dot(grad_mixed, w_out, preferred_element_type=jnp.float32)]
    pallas_call x1, Pallas kernels: 34.8 us -> 39.8 us  [give_back(): pl.pallas_call(functools.partial(return_kernel, n), out_shape=[jax.ShapeD...]
    reshape x3 -> x1, local copies, waits for them, and re-layouts: 2.89 us -> 0.07 us  [body(): grad_mix = grad_mix.astype(jnp.float32).reshape(shape_value)]
    convert_element_type x1 -> x2, other arithmetic: 2.44 us -> 0.25 us  [the longest x1 0.2 us: body(): (place[:, :, None] == jnp.arange(capacity, dtype=jnp.float32)).astype(jnp...]
    reshape x1 -> x0, other arithmetic: 2.16 us -> none  [body(): grad_normed = grad_normed.transpose(1, 0, 2).reshape(tok_count, model_width)]
    reduce_sum x2 -> x0, other arithmetic: 1.68 us -> none  [the longest x1 1.4 us: body(): jnp.mean(grad_unit * unit_rows, axis=-1, keepdims=True)]
where the time goes in v2:
time: 144 us; the launch traced here: 143 us
  Pallas kernels  94.8 us (66%)
  matrix products  22.2 us (15%)
  other arithmetic  12.8 us (9%)
  local copies, waits for them, and re-layouts  11.7 us (8%)
  between operations  1.49 us (1%)
    pallas_call x1, Pallas kernels, give_back(): pl.pallas_call(functools.partial(return_kernel, n), out_shape=[jax.ShapeD...  39.8 us
    pallas_call x1, Pallas kernels, dispatch(): pl.pallas_call(functools.partial(dispatch_kernel, n), out_shape=[full, fu...  38 us
    pallas_call x1, Pallas kernels, last_exchange(): pl.pallas_call(functools.partial(last_kernel, n), out_shape=[jax.ShapeDty...  17.1 us
    unnamed x90, local copies, waits for them, and re-layouts  3.97 us

profile of v2, /device:TPU:0, one launch (start us, length us, event | category | flops | bytes accessed | tf_op | source)
XLA Modules:
  0.0 143.0 jit_solution(13325594322538958508)
XLA Ops:
  0.7 0.8 fusion.54
  1.5 0.1 convolution_select_fusion.2
  1.7 0.7 reduce_max.9
  2.4 0.7 fusion.56
  3.1 0.7 fusion.55
  3.8 0.7 select_reduce_fusion.1
  4.5 0.1 select_reduce_fusion
  4.6 0.1 copy.81.weight_ref
  4.8 1.0 reshape.139
  6.0 0.9 reshape.142
  6.9 0.9 reshape.155
  7.9 0.1 copy.77
  8.0 0.6 slice_bitcast_fusion.2
  8.6 0.3 fusion.50
  8.9 1.3 subtract_exponential_fusion.4
  10.2 0.5 broadcast_multiply_fusion.1
  10.7 0.6 slice_bitcast_fusion.4
  11.4 0.4 copy-done.40
  11.8 0.7 copy.80
  12.5 0.8 pad_maximum_fusion.1.state_ref
  13.4 38.0 %dispatch.1 = (bf16[8,64,2048]{2,1,0:T(8,128)(2,1)S(1)}, bf16[8,64,2048]{2,1,0:T(8,128)(2,1)S(1)}, f32[136,128]{1,0:T(8,128)S(1)}) custom-call(bf16[128,2048]{1,0:T(8,128)(2,1)S(1)} %copy-done.2, bf16[128,2048]{1,0:T(8,128)(2,1)S(1)} %copy-done.3, f32[1,2048]{1,0:T(1,128)S(1)} %bitcast.151, bf16[8,64,128]{2,1,0:T(8,128)(2,1)S(1)} %fusion.23.pick_ref, ...), custom_call_target="tpu_custom_call" | custom-call | tf_op jit(solution)/shard_map/dispatch/pallas_call | solution.py:265
  51.4 1.3 fusion.5
  52.6 0.1 copy-done.13
  52.8 1.2 fusion.8
  54.0 0.2 copy-done.43
  54.2 1.4 %multiply_convert_fusion.1 = (bf16[512,384]{1,0:T(8,128)(2,1)S(1)}, bf16[512,384]{1,0:T(8,128)(2,1)S(1)}) fusion(f32[512,384]{1,0:T(8,128)S(1)} %fusion.5, f32[512,384]{1,0:T(8,128)S(1)} %fusion.8, bf16[512,2048]{1,0:T(8,128)(2,1)S(1)} %bitcast.153, bf16[1,384,2048]{2,1,0:T(8,128)(2,1)S(1)} %copy-done.43), kind=kOutput, calls=%fused_computation.37 | convolution fusion | flops 807862272 | bytes 6029312 | tf_op jit(solution)/shard_map/rd,fd->rf/dot_general | solution.py:726
  55.6 2.5 %fusion = bf16[1,2048,384]{2,1,0:T(8,128)(2,1)} fusion(bf16[512,2048]{1,0:T(8,128)(2,1)S(1)} %bitcast.157, bf16[512,384]{1,0:T(8,128)(2,1)S(1)} %get-tuple-element.25), kind=kOutput, calls=%fused_computation.4 | convolution fusion | flops 806092800 | bytes 4063232 | tf_op jit(solution)/shard_map/rd,rf->df/dot_general | solution.py:731
  58.1 2.4 %fusion.1 = bf16[1,2048,384]{2,1,0:T(8,128)(2,1)} fusion(bf16[512,2048]{1,0:T(8,128)(2,1)S(1)} %bitcast.158, bf16[512,384]{1,0:T(8,128)(2,1)S(1)} %get-tuple-element.24), kind=kOutput, calls=%fused_computation.5 | convolution fusion | flops 806092800 | bytes 4063232 | tf_op jit(solution)/shard_map/rd,rf->df/dot_general | solution.py:734
  60.5 2.2 %fusion.2 = bf16[1,384,2048]{2,1,0:T(8,128)(2,1)} fusion(bf16[512,2048]{1,0:T(8,128)(2,1)S(1)} %bitcast.154, f32[512,384]{1,0:T(8,128)S(1)} %fusion.8, f32[512,384]{1,0:T(8,128)S(1)} %fusion.5), kind=kOutput, calls=%fused_computation.6 | convolution fusion | flops 807272448 | bytes 5242880 | tf_op jit(solution)/shard_map/rf,rd->fd/dot_general | solution.py:725
  62.7 1.3 fusion.3
  64.0 2.6 %add_convert_fusion = bf16[512,2048]{1,0:T(8,128)(2,1)} fusion(f32[512,2048]{1,0:T(8,128)S(1)} %fusion.3, bf16[512,384]{1,0:T(8,128)(2,1)S(1)} %get-tuple-element.24, bf16[1,2048,384]{2,1,0:T(8,128)(2,1)S(1)} %copy-done.13), kind=kOutput, calls=%fused_computation | convolution fusion | flops 807403520 | bytes 8257536 | tf_op jit(solution)/shard_map/rf,df->rd/dot_general | solution.py:738
  66.9 0.1 reshape.157
  67.2 0.4 convolution_bitcast_fusion.5
  67.7 0.5 convolution_select_fusion.1
  68.2 0.3 multiply_reduce_fusion.1
  68.7 0.4 copy-done.10
  69.2 0.2 fusion.22.pick_ref
  69.4 1.2 copy-done.4
  70.6 39.8 %give_back.1 = (bf16[8,128,256]{2,1,0:T(8,128)(2,1)S(1)}, bf16[128,256]{1,0:T(8,128)(2,1)S(1)}, bf16[8,128,256]{2,1,0:T(8,128)(2,1)S(1)}) custom-call(bf16[8,64,2048]{2,1,0:T(8,128)(2,1)S(1)} %bitcast.149, bf16[128,256]{1,0:T(8,128)(2,1)S(1)} %bitcast.150, bf16[8,128,64]{2,1,0:T(8,128)(2,1)S(1)} %fusion.22.pick_ref, bf16[128,2048]{1,0:T(8,128)(2,1)S(1)} %copy-done.2, ...), custom_call_target="tpu_custom_call" | custom-call | tf_op jit(solution)/shard_map/give_back/pallas_call | solution.py:474
  110.4 0.8 copy-done.5
  111.3 1.2 multiply_reduce_fusion
  112.5 1.1 subtract_multiply_fusion
  113.6 1.2 fusion.46
  114.8 0.8 fusion.30
  115.7 0.7 pad_maximum_fusion.state_ref
  116.4 17.1 %last_exchange.1 = (bf16[8,128,256]{2,1,0:T(8,128)(2,1)S(1)}, f32[136,128]{1,0:T(8,128)S(1)}) custom-call(bf16[8,128,256]{2,1,0:T(8,128)(2,1)S(1)} %get-tuple-element.19.rows_ref, f32[136,128]{1,0:T(8,128)S(1)} %pad_maximum_fusion.state_ref), custom_call_target="tpu_custom_call" | custom-call | tf_op jit(solution)/shard_map/last_exchange/pallas_call | solution.py:591
  133.4 1.0 convolution_bitcast_fusion
  134.5 1.3 fusion.16
  135.8 0.2 convolution_select_fusion
  136.0 0.4 fusion.15
  136.7 0.3 fusion.12
  137.0 0.3 multiply_subtract_fusion
  137.4 0.1 copy.98
  137.5 0.7 convert_element_type.74
  138.2 0.1 copy.101
  138.3 0.7 convert_element_type.76
  139.0 0.4 fusion.66
  139.4 0.5 fusion.20
  140.0 0.6 copy.133
  140.6 0.1 copy.107
  140.7 0.1 reshape.153
  140.9 1.1 reduce_window_sum.34
  142.0 0.2 multiply_reduce_fusion.2
  142.3 0.6 broadcast_add_fusion
  (108 shorter events, 1.6 us)
Async XLA Ops:
  0.6 50.7 %copy-start = (bf16[1,2048,384]{2,1,0:T(8,128)(2,1)S(1)}, bf16[1,2048,384]{2,1,0:T(8,128)(2,1)}, u32[]{:S(2)}) copy-start(bf16[1,2048,384]{2,1,0:T(8,128)(2,1)} %param.19) | copy-start | bytes 4718596
  0.6 12.7 %copy-start.2 = (bf16[128,2048]{1,0:T(8,128)(2,1)S(1)}, bf16[128,2048]{1,0:T(8,128)(2,1)}, u32[]{:S(2)}) copy-start(bf16[128,2048]{1,0:T(8,128)(2,1)} %hidden_ref.3) | copy-start | bytes 1572868
  0.7 12.7 %copy-start.3 = (bf16[128,2048]{1,0:T(8,128)(2,1)S(1)}, bf16[128,2048]{1,0:T(8,128)(2,1)}, u32[]{:S(2)}) copy-start(bf16[128,2048]{1,0:T(8,128)(2,1)} %cot_ref.3) | copy-start | bytes 1572868
  0.7 12.7 %copy-start.7 = (f32[2048]{0:T(1024)S(1)}, f32[2048]{0:T(1024)}, u32[]{:S(2)}) copy-start(f32[2048]{0:T(1024)} %param.15) | copy-start | bytes 24580
  1.7 4.3 %copy-start.24 = (f32[8,128]{1,0:T(8,128)}, f32[8,128]{1,0:T(8,128)S(1)}, u32[]{:S(2)}) copy-start(f32[8,128]{1,0:T(8,128)S(1)} %convolution_select_fusion.2) | copy-start | bytes 12292
  5.9 2.7 %copy-start.21 = (f32[2,64,2,64]{3,2,1,0:T(2,128)}, f32[2,64,2,64]{3,2,1,0:T(2,128)S(1)}, u32[]{:S(2)}) copy-start(f32[2,64,2,64]{3,2,1,0:T(2,128)S(1)} %fusion.65) | copy-start | bytes 196612
  5.9 5.4 %copy-start.34 = (f32[2,2,64]{2,1,0:T(2,128)}, f32[2,2,64]{2,1,0:T(2,128)S(1)}, u32[]{:S(2)}) copy-start(f32[2,2,64]{2,1,0:T(2,128)S(1)} %fusion.63) | copy-start | bytes 3076
  6.0 46.6 %copy-start.26 = (f32[8,128]{1,0:T(8,128)}, f32[8,128]{1,0:T(8,128)S(1)}, u32[]{:S(2)}) copy-start(f32[8,128]{1,0:T(8,128)S(1)} %broadcast_in_dim.98) | copy-start | bytes 12292
  8.6 2.7 %copy-start.27 = (f32[2,2,64]{2,1,0:T(2,128)}, f32[2,2,64]{2,1,0:T(2,128)S(1)}, u32[]{:S(2)}) copy-start(f32[2,2,64]{2,1,0:T(2,128)S(1)} %get-tuple-element.30) | copy-start | bytes 3076
  8.8 57.8 %copy-start.11 = (f32[2,2,64,128]{3,2,1,0:T(8,128)}, f32[2,2,64,128]{3,2,1,0:T(8,128)S(1)}, u32[]{:S(2)}) copy-start(f32[2,2,64,128]{3,2,1,0:T(8,128)S(1)} %fusion.50) | copy-start | bytes 393220
  10.2 57.0 %copy-start.32 = (f32[2,2,64]{2,1,0:T(2,128)}, f32[2,2,64]{2,1,0:T(2,128)S(1)}, u32[]{:S(2)}) copy-start(f32[2,2,64]{2,1,0:T(2,128)S(1)} %get-tuple-element.31) | copy-start | bytes 3076
  10.7 0.6 copy-start.36
  11.3 0.5 copy-start.40
  51.4 1.4 copy-start.13
  52.8 1.4 copy-start.43
  64.0 2.7 %copy-start.37 = (f32[2,64]{1,0:T(2,128)S(1)}, f32[2,64]{1,0:T(2,128)}, u32[]{:S(2)}) copy-start(f32[2,64]{1,0:T(2,128)} %copy-done.36) | copy-start | bytes 1540
  64.0 2.9 %copy-start.30 = (bf16[128,128]{1,0:T(8,128)(2,1)S(1)}, bf16[128,128]{1,0:T(8,128)(2,1)}, u32[]{:S(2)}) copy-start(bf16[128,128]{1,0:T(8,128)(2,1)} %param.23) | copy-start | bytes 98308
  64.0 3.6 %copy-start.22 = (f32[2,2,64]{2,1,0:T(2,128)S(1)}, f32[2,2,64]{2,1,0:T(2,128)}, u32[]{:S(2)}) copy-start(f32[2,2,64]{2,1,0:T(2,128)} %get-tuple-element.29) | copy-start | bytes 3076
  66.7 1.8 %copy-start.39 = (f32[256]{0:T(256)S(1)}, f32[256]{0:T(256)}, u32[]{:S(2)}) copy-start(f32[256]{0:T(256)} %param.27) | copy-start | bytes 3076
  66.7 2.5 %copy-start.25 = (f32[8,128]{1,0:T(8,128)S(1)}, f32[8,128]{1,0:T(8,128)}, u32[]{:S(2)}) copy-start(f32[8,128]{1,0:T(8,128)} %copy-done.24) | copy-start | bytes 12292
  66.8 2.4 %copy-start.20 = (f32[1,2,64,128]{3,2,1,0:T(8,128)}, f32[1,2,64,128]{3,2,1,0:T(8,128)S(1)}, u32[]{:S(2)}) copy-start(f32[1,2,64,128]{3,2,1,0:T(8,128)S(1)} %slice_add_fusion.1) | copy-start | bytes 196612
  66.9 0.7 copy-start.16
  67.2 2.0 %copy-start.8 = (f32[2,64,2,64]{1,3,2,0:T(8,128)}, f32[2,64,2,64]{1,3,2,0:T(8,128)S(1)}, u32[]{:S(2)}) copy-start(f32[2,64,2,64]{1,3,2,0:T(8,128)S(1)} %copy.83) | copy-start | bytes 196612
  67.2 2.2 %copy-start.1 = (bf16[512,2048]{1,0:T(8,128)(2,1)S(1)}, bf16[512,2048]{1,0:T(8,128)(2,1)}, u32[]{:S(2)}) copy-start(bf16[512,2048]{1,0:T(8,128)(2,1)} %add_convert_fusion) | copy-start | bytes 6291460
  68.2 1.0 copy-start.14
  68.5 0.7 copy-start.10
  68.5 0.7 copy-start.29
  69.4 1.2 copy-start.4
  110.4 0.8 copy-start.5
  111.2 23.3 %copy-start.17 = (f32[128,128]{0,1:T(8,128)S(1)}, f32[128,128]{0,1:T(8,128)}, u32[]{:S(2)}) copy-start(f32[128,128]{0,1:T(8,128)} %copy-done.16) | copy-start | bytes 196612
  111.2 23.3 %copy-start.33 = (f32[2,2,64]{2,1,0:T(2,128)S(1)}, f32[2,2,64]{2,1,0:T(2,128)}, u32[]{:S(2)}) copy-start(f32[2,2,64]{2,1,0:T(2,128)} %copy-done.32) | copy-start | bytes 3076
  111.2 22.2 %copy-start.6 = (bf16[8,128,256]{2,1,0:T(8,128)(2,1)S(1)}, bf16[8,128,256]{2,1,0:T(8,128)(2,1)}, u32[]{:S(2)}) copy-start(bf16[8,128,256]{2,1,0:T(8,128)(2,1)} %copy-done.5) | copy-start | bytes 1572868
  112.5 23.5 %copy-start.23 = (f32[2,2,64]{2,1,0:T(2,128)S(1)}, f32[2,2,64]{2,1,0:T(2,128)}, u32[]{:S(2)}) copy-start(f32[2,2,64]{2,1,0:T(2,128)} %get-tuple-element.29) | copy-start | bytes 3076
  113.5 22.9 %copy-start.42 = (f32[2,64]{1,0:T(2,128)S(1)}, f32[2,64]{1,0:T(2,128)}, u32[]{:S(2)}) copy-start(f32[2,64]{1,0:T(2,128)} %get-tuple-element.38) | copy-start | bytes 1540
  114.7 0.9 copy-start.18
  115.5 21.2 %copy-start.28 = (f32[2,2,64]{2,1,0:T(2,128)S(1)}, f32[2,2,64]{2,1,0:T(2,128)}, u32[]{:S(2)}) copy-start(f32[2,2,64]{2,1,0:T(2,128)} %copy-done.27) | copy-start | bytes 3076
  115.5 21.2 %copy-start.31 = (f32[2,2,64]{2,1,0:T(2,128)S(1)}, f32[2,2,64]{2,1,0:T(2,128)}, u32[]{:S(2)}) copy-start(f32[2,2,64]{2,1,0:T(2,128)} %get-tuple-element.33) | copy-start | bytes 3076
  116.3 20.1 %copy-start.19 = (f32[2,2,64,128]{3,2,1,0:T(8,128)S(1)}, f32[2,2,64,128]{3,2,1,0:T(8,128)}, u32[]{:S(2)}) copy-start(f32[2,2,64,128]{3,2,1,0:T(8,128)} %copy-done.18) | copy-start | bytes 393220
  116.3 20.6 %copy-start.9 = (f32[2,64,2,64]{1,3,2,0:T(8,128)S(1)}, f32[2,64,2,64]{1,3,2,0:T(8,128)}, u32[]{:S(2)}) copy-start(f32[2,64,2,64]{1,3,2,0:T(8,128)} %copy-done.8) | copy-start | bytes 196612
  134.5 4.5 %copy-start.15 = (f32[2,2,64,64]{3,2,1,0:T(8,128)S(1)}, f32[2,2,64,64]{3,2,1,0:T(8,128)}, u32[]{:S(2)}) copy-start(f32[2,2,64,64]{3,2,1,0:T(8,128)} %copy-done.14) | copy-start | bytes 196612
  136.4 5.5 %copy-start.35 = (f32[2,2,64]{2,1,0:T(2,128)S(1)}, f32[2,2,64]{2,1,0:T(2,128)}, u32[]{:S(2)}) copy-start(f32[2,2,64]{2,1,0:T(2,128)} %copy-done.34) | copy-start | bytes 3076
  136.5 5.5 %copy-start.12 = (f32[2,2,64,128]{3,2,1,0:T(8,128)S(1)}, f32[2,2,64,128]{3,2,1,0:T(8,128)}, u32[]{:S(2)}) copy-start(f32[2,2,64,128]{3,2,1,0:T(8,128)} %copy-done.11) | copy-start | bytes 393220
  136.5 5.5 %copy-start.38 = (f32[2,64]{1,0:T(2,128)S(1)}, f32[2,64]{1,0:T(2,128)}, u32[]{:S(2)}) copy-start(f32[2,64]{1,0:T(2,128)} %copy-done.36) | copy-start | bytes 1540
  136.5 5.5 %copy-start.41 = (f32[2,64]{1,0:T(2,128)S(1)}, f32[2,64]{1,0:T(2,128)}, u32[]{:S(2)}) copy-start(f32[2,64]{1,0:T(2,128)} %copy-done.40) | copy-start | bytes 1540

commit v3 on v2

--- a/solution.py
+++ b/solution.py
@@ -678,12 +678,14 @@
     ones_decay = jnp.ones_like(total_log)
     local_end, local_start = block_scan(block_decay, block_kv, zero_state, False)
     sp_count = lax.axis_size("sp")
-    route_weight = jax.nn.softmax(route_logits, axis=-1)
     expert_count = sp_count
     capacity = 4 * tok_count // expert_count
-    named = route_ids[:, :, None] == jnp.arange(expert_count, dtype=jnp.int32)[None, None, :]
-    names = jnp.any(named, axis=1)
-    weight_of = jnp.sum(jnp.where(named, route_weight[:, :, None], 0.0), axis=1)
+    experts = jnp.arange(expert_count, dtype=jnp.int32)[None, :]
+    first, second = route_ids[:, :1] == experts, route_ids[:, 1:] == experts
+    names = first | second
+    margin = route_logits[:, :1] - route_logits[:, 1:]
+    weight_of = jnp.where(first, margin, jnp.where(second, -margin, 0.0))
+    weight_of = jnp.where(names, jax.nn.sigmoid(weight_of), 0.0)
     before = (jnp.arange(tok_count)[:, None] > jnp.arange(tok_count)[None, :]).astype(jnp.bfloat16)
     rank = jnp.dot(before, names.astype(jnp.bfloat16), preferred_element_type=jnp.float32)
     place = jnp.where(names, rank, -1.0).T

time: 144 us -> 144 us (level)
    unnamed x90 -> x86, local copies, waits for them, and re-layouts: 3.97 us -> 4.18 us
where the time goes in v3:
time: 144 us
  Pallas kernels  94.8 us (66%)
  matrix products  23.2 us (16%)
  local copies, waits for them, and re-layouts  12.8 us (9%)
  other arithmetic  11.4 us (8%)
  between operations  1.49 us (1%)
    pallas_call x1, Pallas kernels, give_back(): pl.pallas_call(functools.partial(return_kernel, n), out_shape=[jax.ShapeD...  39.8 us
    pallas_call x1, Pallas kernels, dispatch(): pl.pallas_call(functools.partial(dispatch_kernel, n), out_shape=[full, fu...  38 us
    pallas_call x1, Pallas kernels, last_exchange(): pl.pallas_call(functools.partial(last_kernel, n), out_shape=[jax.ShapeDty...  17.1 us
    unnamed x86, local copies, waits for them, and re-layouts  4.18 us

profile of v3, /device:TPU:0, one launch (start us, length us, event | category | flops | bytes accessed | tf_op | source)
XLA Modules:
  0.0 143.6 jit_solution(3020324392117849729)
XLA Ops:
  0.7 0.8 slice_bitcast_fusion.8
  1.5 0.2 convolution_select_fusion.2
  1.8 0.8 fusion.66
  2.6 0.2 select_reduce_fusion
  2.8 0.1 copy.46.weight_ref
  2.9 1.0 reshape.206
  4.1 0.9 reshape.209
  5.0 0.9 reshape.222
  6.0 0.1 copy.42
  6.1 0.6 slice_bitcast_fusion.2
  6.7 0.3 fusion.52
  7.0 1.3 subtract_exponential_fusion.4
  8.3 0.6 broadcast_multiply_fusion.1
  8.9 0.6 slice_bitcast_fusion.4
  9.5 0.1 fusion.31
  9.6 0.5 copy-done.38
  10.0 0.7 copy.45
  10.8 0.8 pad_maximum_fusion.1.state_ref
  11.6 38.0 %dispatch.1 = (bf16[8,64,2048]{2,1,0:T(8,128)(2,1)S(1)}, bf16[8,64,2048]{2,1,0:T(8,128)(2,1)S(1)}, f32[136,128]{1,0:T(8,128)S(1)}) custom-call(bf16[128,2048]{1,0:T(8,128)(2,1)S(1)} %copy-done.2, bf16[128,2048]{1,0:T(8,128)(2,1)S(1)} %copy-done.3, f32[1,2048]{1,0:T(1,128)S(1)} %bitcast.155, bf16[8,64,128]{2,1,0:T(8,128)(2,1)S(1)} %fusion.23.pick_ref, ...), custom_call_target="tpu_custom_call" | custom-call | tf_op jit(solution)/shard_map/dispatch/pallas_call | solution.py:265
  49.6 1.3 fusion.5
  50.9 0.1 copy-done.13
  51.0 1.2 fusion.8
  52.2 0.2 copy-done.41
  52.4 1.4 multiply_convert_fusion.1
  53.8 2.5 %fusion = bf16[1,2048,384]{2,1,0:T(8,128)(2,1)} fusion(bf16[512,2048]{1,0:T(8,128)(2,1)S(1)} %bitcast.161, bf16[512,384]{1,0:T(8,128)(2,1)S(1)} %get-tuple-element.25), kind=kOutput, calls=%fused_computation.4 | convolution fusion | flops 806092800 | bytes 4063232 | tf_op jit(solution)/shard_map/rd,rf->df/dot_general | solution.py:733
  56.3 2.4 %fusion.1 = bf16[1,2048,384]{2,1,0:T(8,128)(2,1)} fusion(bf16[512,2048]{1,0:T(8,128)(2,1)S(1)} %bitcast.162, bf16[512,384]{1,0:T(8,128)(2,1)S(1)} %get-tuple-element.24), kind=kOutput, calls=%fused_computation.5 | convolution fusion | flops 806092800 | bytes 4063232 | tf_op jit(solution)/shard_map/rd,rf->df/dot_general | solution.py:736
  58.7 2.2 %fusion.2 = bf16[1,384,2048]{2,1,0:T(8,128)(2,1)} fusion(bf16[512,2048]{1,0:T(8,128)(2,1)S(1)} %bitcast.158, f32[512,384]{1,0:T(8,128)S(1)} %fusion.8, f32[512,384]{1,0:T(8,128)S(1)} %fusion.5), kind=kOutput, calls=%fused_computation.6 | convolution fusion | flops 807272448 | bytes 5242880 | tf_op jit(solution)/shard_map/rf,rd->fd/dot_general | solution.py:727
  61.0 1.3 fusion.3
  62.3 2.6 %add_convert_fusion = bf16[512,2048]{1,0:T(8,128)(2,1)} fusion(f32[512,2048]{1,0:T(8,128)S(1)} %fusion.3, bf16[512,384]{1,0:T(8,128)(2,1)S(1)} %get-tuple-element.24, bf16[1,2048,384]{2,1,0:T(8,128)(2,1)S(1)} %copy-done.13), kind=kOutput, calls=%fused_computation | convolution fusion | flops 807403520 | bytes 8257536 | tf_op jit(solution)/shard_map/rf,df->rd/dot_general | solution.py:740
  65.1 0.1 reshape.224
  65.3 0.1 copy.48
  65.4 0.4 convolution_bitcast_fusion.5
  65.9 1.4 convolution_select_fusion.1
  67.3 0.3 multiply_reduce_fusion.1
  67.6 0.6 copy-done.28
  68.2 0.8 multiply_convert_fusion.4
  69.1 0.9 fusion.22.pick_ref
  70.0 1.2 copy-done.4
  71.3 39.8 %give_back.1 = (bf16[8,128,256]{2,1,0:T(8,128)(2,1)S(1)}, bf16[128,256]{1,0:T(8,128)(2,1)S(1)}, bf16[8,128,256]{2,1,0:T(8,128)(2,1)S(1)}) custom-call(bf16[8,64,2048]{2,1,0:T(8,128)(2,1)S(1)} %bitcast.153, bf16[128,256]{1,0:T(8,128)(2,1)S(1)} %bitcast.154, bf16[8,128,64]{2,1,0:T(8,128)(2,1)S(1)} %fusion.22.pick_ref, bf16[128,2048]{1,0:T(8,128)(2,1)S(1)} %copy-done.2, ...), custom_call_target="tpu_custom_call" | custom-call | tf_op jit(solution)/shard_map/give_back/pallas_call | solution.py:474
  111.0 0.8 copy-done.5
  111.9 1.2 multiply_reduce_fusion
  113.1 1.1 subtract_multiply_fusion
  114.2 1.2 fusion.48
  115.4 0.8 fusion.30
  116.3 0.7 pad_maximum_fusion.state_ref
  117.0 17.1 %last_exchange.1 = (bf16[8,128,256]{2,1,0:T(8,128)(2,1)S(1)}, f32[136,128]{1,0:T(8,128)S(1)}) custom-call(bf16[8,128,256]{2,1,0:T(8,128)(2,1)S(1)} %get-tuple-element.19.rows_ref, f32[136,128]{1,0:T(8,128)S(1)} %pad_maximum_fusion.state_ref), custom_call_target="tpu_custom_call" | custom-call | tf_op jit(solution)/shard_map/last_exchange/pallas_call | solution.py:591
  134.0 1.0 convolution_bitcast_fusion
  135.1 1.3 fusion.16
  136.4 0.2 convolution_select_fusion
  136.6 0.4 fusion.15
  137.3 0.3 fusion.12
  137.6 0.3 multiply_subtract_fusion
  138.0 0.1 copy.63
  138.1 0.7 convert_element_type.74
  138.8 0.1 copy.66
  138.9 0.7 convert_element_type.76
  139.6 0.4 fusion.70
  140.0 0.5 fusion.20
  140.6 0.6 copy.98
  141.2 0.1 copy.72
  141.3 0.1 reshape.220
  141.5 1.1 reduce_window_sum.34
  142.7 0.2 multiply_reduce_fusion.2
  142.9 0.6 broadcast_add_fusion
  (102 shorter events, 1.3 us)
Async XLA Ops:
  0.6 48.9 %copy-start = (bf16[1,2048,384]{2,1,0:T(8,128)(2,1)S(1)}, bf16[1,2048,384]{2,1,0:T(8,128)(2,1)}, u32[]{:S(2)}) copy-start(bf16[1,2048,384]{2,1,0:T(8,128)(2,1)} %param.19) | copy-start | bytes 4718596
  0.6 11.0 %copy-start.2 = (bf16[128,2048]{1,0:T(8,128)(2,1)S(1)}, bf16[128,2048]{1,0:T(8,128)(2,1)}, u32[]{:S(2)}) copy-start(bf16[128,2048]{1,0:T(8,128)(2,1)} %hidden_ref.3) | copy-start | bytes 1572868
  0.7 10.9 %copy-start.3 = (bf16[128,2048]{1,0:T(8,128)(2,1)S(1)}, bf16[128,2048]{1,0:T(8,128)(2,1)}, u32[]{:S(2)}) copy-start(bf16[128,2048]{1,0:T(8,128)(2,1)} %cot_ref.3) | copy-start | bytes 1572868
  0.7 10.9 %copy-start.7 = (f32[2048]{0:T(1024)S(1)}, f32[2048]{0:T(1024)}, u32[]{:S(2)}) copy-start(f32[2048]{0:T(1024)} %param.15) | copy-start | bytes 24580
  1.8 1.0 copy-start.24
  4.0 2.7 %copy-start.22 = (f32[2,64,2,64]{3,2,1,0:T(2,128)}, f32[2,64,2,64]{3,2,1,0:T(2,128)S(1)}, u32[]{:S(2)}) copy-start(f32[2,64,2,64]{3,2,1,0:T(2,128)S(1)} %fusion.69) | copy-start | bytes 196612
  4.0 5.4 %copy-start.33 = (f32[2,2,64]{2,1,0:T(2,128)}, f32[2,2,64]{2,1,0:T(2,128)S(1)}, u32[]{:S(2)}) copy-start(f32[2,2,64]{2,1,0:T(2,128)S(1)} %fusion.67) | copy-start | bytes 3076
  4.1 46.7 %copy-start.25 = (f32[8,128]{1,0:T(8,128)}, f32[8,128]{1,0:T(8,128)S(1)}, u32[]{:S(2)}) copy-start(f32[8,128]{1,0:T(8,128)S(1)} %broadcast_in_dim.110) | copy-start | bytes 12292
  6.7 2.8 %copy-start.26 = (f32[2,2,64]{2,1,0:T(2,128)}, f32[2,2,64]{2,1,0:T(2,128)S(1)}, u32[]{:S(2)}) copy-start(f32[2,2,64]{2,1,0:T(2,128)S(1)} %get-tuple-element.30) | copy-start | bytes 3076
  7.0 57.9 %copy-start.11 = (f32[2,2,64,128]{3,2,1,0:T(8,128)}, f32[2,2,64,128]{3,2,1,0:T(8,128)S(1)}, u32[]{:S(2)}) copy-start(f32[2,2,64,128]{3,2,1,0:T(8,128)S(1)} %fusion.52) | copy-start | bytes 393220
  8.3 57.1 %copy-start.31 = (f32[2,2,64]{2,1,0:T(2,128)}, f32[2,2,64]{2,1,0:T(2,128)S(1)}, u32[]{:S(2)}) copy-start(f32[2,2,64]{2,1,0:T(2,128)S(1)} %get-tuple-element.31) | copy-start | bytes 3076
  8.9 0.6 copy-start.35
  9.5 0.6 copy-start.38
  49.6 1.4 copy-start.13
  51.0 1.4 copy-start.41
  62.2 2.7 %copy-start.36 = (f32[2,64]{1,0:T(2,128)S(1)}, f32[2,64]{1,0:T(2,128)}, u32[]{:S(2)}) copy-start(f32[2,64]{1,0:T(2,128)} %copy-done.35) | copy-start | bytes 1540
  62.3 2.9 %copy-start.29 = (bf16[128,128]{1,0:T(8,128)(2,1)S(1)}, bf16[128,128]{1,0:T(8,128)(2,1)}, u32[]{:S(2)}) copy-start(bf16[128,128]{1,0:T(8,128)(2,1)} %param.23) | copy-start | bytes 98308
  65.0 4.1 %copy-start.21 = (f32[1,2,64,128]{3,2,1,0:T(8,128)}, f32[1,2,64,128]{3,2,1,0:T(8,128)S(1)}, u32[]{:S(2)}) copy-start(f32[1,2,64,128]{3,2,1,0:T(8,128)S(1)} %slice_add_fusion.1) | copy-start | bytes 196612
  65.1 0.7 copy-start.16
  65.4 3.7 %copy-start.8 = (f32[2,64,2,64]{1,3,2,0:T(8,128)}, f32[2,64,2,64]{1,3,2,0:T(8,128)S(1)}, u32[]{:S(2)}) copy-start(f32[2,64,2,64]{1,3,2,0:T(8,128)S(1)} %copy.48) | copy-start | bytes 196612
  65.4 4.6 %copy-start.1 = (bf16[512,2048]{1,0:T(8,128)(2,1)S(1)}, bf16[512,2048]{1,0:T(8,128)(2,1)}, u32[]{:S(2)}) copy-start(bf16[512,2048]{1,0:T(8,128)(2,1)} %add_convert_fusion) | copy-start | bytes 6291460
  67.3 1.9 %copy-start.14 = (f32[2,2,64,64]{3,2,1,0:T(8,128)}, f32[2,2,64,64]{3,2,1,0:T(8,128)S(1)}, u32[]{:S(2)}) copy-start(f32[2,2,64,64]{3,2,1,0:T(8,128)S(1)} %convolution_select_fusion.1) | copy-start | bytes 196612
  67.6 1.5 %copy-start.10 = (f32[2,64,2,128]{3,1,2,0:T(8,128)}, f32[2,64,2,128]{3,1,2,0:T(8,128)S(1)}, u32[]{:S(2)}) copy-start(f32[2,64,2,128]{3,1,2,0:T(8,128)S(1)} %get-tuple-element.45) | copy-start | bytes 393220
  67.6 0.6 copy-start.28
  70.0 1.2 copy-start.4
  111.0 0.8 copy-start.5
  111.8 23.3 %copy-start.17 = (f32[128,128]{0,1:T(8,128)S(1)}, f32[128,128]{0,1:T(8,128)}, u32[]{:S(2)}) copy-start(f32[128,128]{0,1:T(8,128)} %copy-done.16) | copy-start | bytes 196612
  111.8 23.3 %copy-start.32 = (f32[2,2,64]{2,1,0:T(2,128)S(1)}, f32[2,2,64]{2,1,0:T(2,128)}, u32[]{:S(2)}) copy-start(f32[2,2,64]{2,1,0:T(2,128)} %copy-done.31) | copy-start | bytes 3076
  111.8 22.2 %copy-start.6 = (bf16[8,128,256]{2,1,0:T(8,128)(2,1)S(1)}, bf16[8,128,256]{2,1,0:T(8,128)(2,1)}, u32[]{:S(2)}) copy-start(bf16[8,128,256]{2,1,0:T(8,128)(2,1)} %copy-done.5) | copy-start | bytes 1572868
  113.1 23.5 %copy-start.23 = (f32[2,2,64]{2,1,0:T(2,128)S(1)}, f32[2,2,64]{2,1,0:T(2,128)}, u32[]{:S(2)}) copy-start(f32[2,2,64]{2,1,0:T(2,128)} %get-tuple-element.29) | copy-start | bytes 3076
  114.2 22.9 %copy-start.40 = (f32[2,64]{1,0:T(2,128)S(1)}, f32[2,64]{1,0:T(2,128)}, u32[]{:S(2)}) copy-start(f32[2,64]{1,0:T(2,128)} %get-tuple-element.38) | copy-start | bytes 1540
  115.4 0.9 copy-start.19
  116.2 21.2 %copy-start.27 = (f32[2,2,64]{2,1,0:T(2,128)S(1)}, f32[2,2,64]{2,1,0:T(2,128)}, u32[]{:S(2)}) copy-start(f32[2,2,64]{2,1,0:T(2,128)} %copy-done.26) | copy-start | bytes 3076
  116.2 21.2 %copy-start.30 = (f32[2,2,64]{2,1,0:T(2,128)S(1)}, f32[2,2,64]{2,1,0:T(2,128)}, u32[]{:S(2)}) copy-start(f32[2,2,64]{2,1,0:T(2,128)} %get-tuple-element.33) | copy-start | bytes 3076
  117.0 20.1 %copy-start.20 = (f32[2,2,64,128]{3,2,1,0:T(8,128)S(1)}, f32[2,2,64,128]{3,2,1,0:T(8,128)}, u32[]{:S(2)}) copy-start(f32[2,2,64,128]{3,2,1,0:T(8,128)} %copy-done.19) | copy-start | bytes 393220
  117.0 20.6 %copy-start.9 = (f32[2,64,2,64]{1,3,2,0:T(8,128)S(1)}, f32[2,64,2,64]{1,3,2,0:T(8,128)}, u32[]{:S(2)}) copy-start(f32[2,64,2,64]{1,3,2,0:T(8,128)} %copy-done.8) | copy-start | bytes 196612
  135.1 4.5 %copy-start.15 = (f32[2,2,64,64]{3,2,1,0:T(8,128)S(1)}, f32[2,2,64,64]{3,2,1,0:T(8,128)}, u32[]{:S(2)}) copy-start(f32[2,2,64,64]{3,2,1,0:T(8,128)} %copy-done.14) | copy-start | bytes 196612
  137.1 5.5 %copy-start.34 = (f32[2,2,64]{2,1,0:T(2,128)S(1)}, f32[2,2,64]{2,1,0:T(2,128)}, u32[]{:S(2)}) copy-start(f32[2,2,64]{2,1,0:T(2,128)} %copy-done.33) | copy-start | bytes 3076
  137.1 5.6 %copy-start.12 = (f32[2,2,64,128]{3,2,1,0:T(8,128)S(1)}, f32[2,2,64,128]{3,2,1,0:T(8,128)}, u32[]{:S(2)}) copy-start(f32[2,2,64,128]{3,2,1,0:T(8,128)} %copy-done.11) | copy-start | bytes 393220
  137.1 5.6 %copy-start.18 = (f32[128,128]{0,1:T(8,128)S(1)}, f32[128,128]{0,1:T(8,128)}, u32[]{:S(2)}) copy-start(f32[128,128]{0,1:T(8,128)} %copy-done.16) | copy-start | bytes 196612
  137.1 5.6 %copy-start.37 = (f32[2,64]{1,0:T(2,128)S(1)}, f32[2,64]{1,0:T(2,128)}, u32[]{:S(2)}) copy-start(f32[2,64]{1,0:T(2,128)} %copy-done.35) | copy-start | bytes 1540
  137.1 5.6 %copy-start.39 = (f32[2,64]{1,0:T(2,128)S(1)}, f32[2,64]{1,0:T(2,128)}, u32[]{:S(2)}) copy-start(f32[2,64]{1,0:T(2,128)} %copy-done.38) | copy-start | bytes 1540
